TPU v7x, 32 devices: a whole 2x2x4 slice. The times are simulated.
32 devices in a mesh: ep: 8 (over z, x), tp: 4 (over y, core).
Axes of the slice: x: 2, y: 2, z: 4, core: 2. Of those that a mesh axis runs over, the one named last changes fastest.
Arguments:
- x_path: bfloat16 [8192, 2048], P('ep', 'tp'), may hold values from -6 to 6
- gate_path: bfloat16 [8192, 2048], P('ep', 'tp'), may hold values from -6 to 6
- conv_taps: float32 [4, 2048], P(None, 'tp'), may hold values from -3 to 3
- decay_gate_w: bfloat16 [2, 16, 128, 128], P(None, 'tp'), may hold values from -0.5 to 0.5
- input_gate_w: bfloat16 [2, 16, 128, 128], P(None, 'tp'), may hold values from -0.5 to 0.5
- decay_rate: float32 [2, 2048], P(None, 'tp'), may hold values from 0 to 1, as said below
- decay_shift: float32 [8192, 16], P('ep', 'tp'), may hold values from -1 to 0, as said below
- expert_in: bfloat16 [512, 2048], P('ep'), may hold values from -6 to 6
- norm_gain: float32 [2048], replicated, may hold values from 0.1 to 1.9
- routes: int32 [512, 2], P('ep'), may hold values from 0 to 7, all different within a row; in each aligned block of 16 rows (0 to 15, 16 to 31, ...) at most 8 rows name the same one
- route_scores: float32 [512, 2], P('ep'), may hold values from 0.1 to 1
- gate_weight: bfloat16 [8, 2048, 4096], P('ep', None, 'tp'), may hold values from -0.125 to 0.125
- up_weight: bfloat16 [8, 2048, 4096], P('ep', None, 'tp'), may hold values from -0.125 to 0.125
- down_weight: bfloat16 [8, 4096, 2048], P('ep', 'tp'), may hold values from -0.09375 to 0.09375
Outputs:
- recurrent_out: bfloat16 [8192, 2048], P('ep', 'tp')
- expert_out: bfloat16 [512, 2048], P(('ep', 'tp'))
Inputs may be any that keep to these rules, and one draw needn't show every extreme that they name: `routes`: in each aligned block of 16 rows no expert is named by more than 8 rows, and in some block some expert is named by exactly 8 rows; each row names 2 different experts. `decay_rate`: positive rates. `decay_shift`: never positive.
All inputs are finite; a program needn't handle non-finite values.
Results may differ from a plain program's by a relative error of at most 0.019.
Values may be sent and summed in bfloat16 or wider, within the bound.
No kernel may reach another device: no remote copies, remote signals or barrier semaphores. Data moves between devices by JAX's collectives and lax.ppermute only.
A program may use at most 128 MiB of HBM per device.

v0:
```python
import functools
import math

import jax
import jax.numpy as jnp
from jax import lax
from jax.experimental import pallas as pl
from jax.experimental.pallas import tpu as pltpu
from jax.sharding import Mesh
from jax.sharding import PartitionSpec as P

TOP_K = 2
EPSILON = 1e-06
LANES = 128
CHUNKS = 8
STEPS = 32
LOG2E = math.log2(math.e)
LN2 = math.log(2.0)
SERIES = (-2.0 * LN2, -((2.0 * LN2) ** 2) / 2.0, -((2.0 * LN2) ** 3) / 6.0)


def far(x):
    return pltpu.with_memory_space_constraint(x, pltpu.HBM)


def gates_kernel(first, fetched, filled, *refs):
    x_ref, gate_ref, before_ref, after_ref, taps_ref, decay_w_ref, input_w_ref, rate_ref, shift_ref = refs[:9]
    at = 9
    sources = refs[at : at + fetched]
    at += fetched + filled
    local_ref, forward_ref, backward_ref, chunk_ref, total_ref = refs[at : at + 5]
    at += 5
    targets = refs[at : at + fetched]
    at += fetched
    rows_ref, decay_ref, drive_ref, state_ref, prod_ref, sems = refs[at:]
    length = x_ref.shape[0]
    per = length // CHUNKS
    pitch = per + 4
    f32 = jnp.float32

    fetches = [
        pltpu.make_async_copy(a.at[0], b, sems.at[i])
        for i, (a, b) in enumerate(zip(sources, targets))
    ]

    @pl.when(pl.program_id(0) == 0)
    def _():
        for fetch in fetches:
            fetch.start()

    for s in range(CHUNKS):
        block = x_ref[s * per : (s + 1) * per, :].astype(f32)
        rows_ref[s * pitch + 2 : s * pitch + 2 + per, :] = block
        if s + 1 < CHUNKS:
            rows_ref[(s + 1) * pitch : (s + 1) * pitch + 2, :] = block[per - 2 : per]
        if s > 0:
            rows_ref[(s - 1) * pitch + per + 2 : (s - 1) * pitch + per + 3, :] = block[0:1]
    rows_ref[0:2, :] = before_ref[...].astype(f32)
    last = (CHUNKS - 1) * pitch + per + 2
    rows_ref[last : last + 1, :] = after_ref[0:1, :].astype(f32)

    taps = [jnp.broadcast_to(taps_ref[k : k + 1, :], (CHUNKS, LANES)) for k in range(4)]
    weights = jnp.concatenate(
        [decay_w_ref[0, 0], input_w_ref[0, 0], decay_w_ref[1, 0], input_w_ref[1, 0]], axis=1
    )
    head = pl.program_id(0) + first
    here = lax.broadcasted_iota(jnp.int32, shift_ref.shape, 0) == head
    shift = jnp.sum(jnp.where(here, shift_ref[...], 0.0), axis=0, keepdims=True) * LOG2E
    shift = jnp.concatenate([shift[:, s * per : (s + 1) * per] for s in range(CHUNKS)], axis=0)
    slopes = [rate_ref[d : d + 1, :] * (-4.0 * LOG2E) for d in range(2)]
    size = STEPS * CHUNKS

    def gates(b, carry):
        state, prod = carry
        base = b * STEPS
        taken = [rows_ref[pl.ds(base + i, CHUNKS, stride=pitch), :] for i in range(STEPS + 3)]
        sums = []
        for i in range(STEPS):
            total = taken[i] * taps[0]
            for k in range(1, 4):
                total = total + taken[i + k] * taps[k]
            sums.append(total)
        conv = jnp.concatenate(sums, axis=0).astype(jnp.bfloat16)
        wide = jnp.dot(conv * jnp.bfloat16(0.5), weights, preferred_element_type=f32)
        half = conv.astype(f32) * 0.5
        turned = pltpu.roll(shift, lax.rem(per - base, per), axis=1)
        moved = jnp.concatenate(
            [jnp.broadcast_to(turned[:, i : i + 1], (CHUNKS, LANES)) for i in range(STEPS)], axis=0
        )
        start = pl.multiple_of(b * size, size)
        for d in range(2):
            decay_t = jnp.tanh(wide[:, 2 * d * LANES : (2 * d + 1) * LANES])
            input_t = jnp.tanh(wide[:, (2 * d + 1) * LANES : (2 * d + 2) * LANES])
            power = slopes[d] * decay_t + (moved + slopes[d])
            decay = jnp.exp2(power)
            small = power * (SERIES[0] + power * (SERIES[1] + power * SERIES[2]))
            lost = jnp.where(power > -0.03125, small, 1.0 - decay * decay)
            root = lost * lax.rsqrt(jnp.maximum(lost, 1e-37))
            drive = root * (input_t + 1.0) * half
            if d == 0:
                for i in range(STEPS):
                    step = decay[i * CHUNKS : (i + 1) * CHUNKS]
                    state = step * state + drive[i * CHUNKS : (i + 1) * CHUNKS]
                    prod = step * prod
                    at = pl.ds(start + i * CHUNKS, CHUNKS)
                    state_ref[at, :] = state
                    row = pl.ds(base + i, CHUNKS, stride=pitch)
                    prod_ref[0, row, :] = prod
            else:
                decay_ref[pl.ds(start, size), :] = decay
                drive_ref[pl.ds(start, size), :] = drive
        return state, prod

    zero = jnp.zeros((CHUNKS, LANES), f32)
    one = jnp.ones((CHUNKS, LANES), f32)
    blocks = per // STEPS
    forward_end, forward_prod = lax.fori_loop(0, blocks, gates, (zero, one))

    def back(b, carry):
        state, prod = carry
        base = per - (b + 1) * STEPS
        start = pl.multiple_of(base * CHUNKS, size)
        for i in reversed(range(STEPS)):
            at = pl.ds(start + i * CHUNKS, CHUNKS)
            step = decay_ref[at, :]
            state = step * state + drive_ref[at, :]
            prod = step * prod
            row = pl.ds(base + i, CHUNKS, stride=pitch)
            rows_ref[row, :] = state + state_ref[at, :]
            prod_ref[1, row, :] = prod
        return state, prod

    backward_end, backward_prod = lax.fori_loop(0, blocks, back, (zero, one))

    chunk_ref[0] = forward_prod
    chunk_ref[1] = forward_end
    chunk_ref[2] = backward_prod
    chunk_ref[3] = backward_end
    state, prod = zero[0:1], one[0:1]
    for s in range(CHUNKS):
        state = forward_prod[s : s + 1] * state + forward_end[s : s + 1]
        prod = prod * forward_prod[s : s + 1]
    total_ref[0:1, :] = prod
    total_ref[1:2, :] = state
    state, prod = zero[0:1], one[0:1]
    for s in reversed(range(CHUNKS)):
        state = backward_prod[s : s + 1] * state + backward_end[s : s + 1]
        prod = prod * backward_prod[s : s + 1]
    total_ref[2:3, :] = prod
    total_ref[3:4, :] = state

    span = 64

    def finish(b, none):
        s = b // (per // span)
        inner = (b % (per // span)) * span
        nat = pl.ds(pl.multiple_of(b * span, span), span)
        row = pl.ds(s * pitch + inner, span)
        g = gate_ref[nat, :].astype(f32)
        gelu = 0.5 * g * (1.0 + jnp.tanh(math.sqrt(2.0 / math.pi) * (g + 0.044715 * (g * g * g))))
        local_ref[nat, :] = (rows_ref[row, :] * gelu).astype(local_ref.dtype)
        forward_ref[nat, :] = (prod_ref[0, row, :] * gelu).astype(forward_ref.dtype)
        backward_ref[nat, :] = (prod_ref[1, row, :] * gelu).astype(backward_ref.dtype)
        return none

    lax.fori_loop(0, length // span, finish, 0)

    @pl.when(pl.program_id(0) == pl.num_programs(0) - 1)
    def _():
        for fetch in fetches:
            fetch.wait()


def local_recurrence(first, count, arrays, weights, partial):
    x, gate, before, after, taps, decay_w, input_w, rate, shift = arrays
    length, channels = x.shape
    heads = decay_w.shape[1]
    per = length // CHUNKS
    pitch = per + 4
    col = lambda h: (0, h + first)
    bf16, f32 = jnp.bfloat16, jnp.float32
    any_ref = pl.BlockSpec(memory_space=pltpu.HBM)
    outs = pl.pallas_call(
        functools.partial(gates_kernel, first, len(weights), len(partial)),
        grid=(count,),
        in_specs=[
            pl.BlockSpec((length, LANES), col),
            pl.BlockSpec((length, LANES), col),
            pl.BlockSpec((2, LANES), col),
            pl.BlockSpec((2, LANES), col),
            pl.BlockSpec((4, LANES), col),
            pl.BlockSpec((2, 1, LANES, LANES), lambda h: (0, h + first, 0, 0)),
            pl.BlockSpec((2, 1, LANES, LANES), lambda h: (0, h + first, 0, 0)),
            pl.BlockSpec((2, LANES), col),
            pl.BlockSpec((heads, length), lambda h: (0, 0)),
        ]
        + [any_ref] * (len(weights) + len(partial)),
        out_specs=[
            pl.BlockSpec((length, LANES), col),
            pl.BlockSpec((length, LANES), col),
            pl.BlockSpec((length, LANES), col),
            pl.BlockSpec((4, CHUNKS, LANES), lambda h: (0, 0, h + first)),
            pl.BlockSpec((4, LANES), col),
        ]
        + [pl.BlockSpec(memory_space=pltpu.VMEM)] * len(weights),
        out_shape=[
            pltpu.HBM((length, channels), bf16),
            pltpu.HBM((length, channels), bf16),
            pltpu.HBM((length, channels), bf16),
            pltpu.HBM((4, CHUNKS, channels), f32),
            pltpu.HBM((4, channels), f32),
        ]
        + [pltpu.VMEM(w.shape[1:], w.dtype) for w in weights],
        scratch_shapes=[
            pltpu.VMEM((CHUNKS * pitch, LANES), f32),
            pltpu.VMEM((length, LANES), f32),
            pltpu.VMEM((length, LANES), f32),
            pltpu.VMEM((length, LANES), f32),
            pltpu.VMEM((2, CHUNKS * pitch, LANES), f32),
            pltpu.SemaphoreType.DMA((3,)),
        ],
        input_output_aliases={9 + len(weights) + i: i for i in range(len(partial))},
        compiler_params=pltpu.CompilerParams(vmem_limit_bytes=20 << 20),
        name="recurrence",
    )(
        far(x), far(gate), before, after, far(taps), far(decay_w), far(input_w), far(rate), far(shift.T),
        *map(far, weights), *map(far, partial)
    )
    return list(outs[:5]), list(outs[5:])


def carry_kernel(place_ref, local_ref, forward_ref, backward_ref, chunk_ref, *refs):
    *pieces, out_ref, all_ref = refs
    length = local_ref.shape[0]
    per = length // CHUNKS
    f32 = jnp.float32
    place = place_ref[0]
    count = 0
    for piece in pieces:
        all_ref[count : count + piece.shape[0]] = piece[...]
        count += piece.shape[0]
    carry = jnp.zeros((1, LANES), f32)
    for e in range(count):
        after = all_ref[e ^ place, 0:1] * carry + all_ref[e ^ place, 1:2]
        carry = jnp.where(e < place, after, carry)
    ahead = [None] * CHUNKS
    for s in range(CHUNKS):
        ahead[s] = carry
        carry = chunk_ref[0, s : s + 1] * carry + chunk_ref[1, s : s + 1]
    carry = jnp.zeros((1, LANES), f32)
    for e in reversed(range(count)):
        after = all_ref[e ^ place, 2:3] * carry + all_ref[e ^ place, 3:4]
        carry = jnp.where(e > place, after, carry)
    behind = [None] * CHUNKS
    for s in reversed(range(CHUNKS)):
        behind[s] = carry
        carry = chunk_ref[2, s : s + 1] * carry + chunk_ref[3, s : s + 1]
    for s in range(CHUNKS):
        at = slice(s * per, (s + 1) * per)
        out_ref[at, :] = (
            local_ref[at, :].astype(f32)
            + forward_ref[at, :].astype(f32) * ahead[s]
            + backward_ref[at, :].astype(f32) * behind[s]
        ).astype(out_ref.dtype)


def add_carries(place, local, forward, backward, chunks, everyone):
    length, channels = local.shape
    count = sum(piece.shape[0] for piece in everyone)
    col = lambda h, p: (0, h)
    return pl.pallas_call(
        carry_kernel,
        grid_spec=pltpu.PrefetchScalarGridSpec(
            num_scalar_prefetch=1,
            grid=(channels // LANES,),
            in_specs=[
                pl.BlockSpec((length, LANES), col),
                pl.BlockSpec((length, LANES), col),
                pl.BlockSpec((length, LANES), col),
                pl.BlockSpec((4, CHUNKS, LANES), lambda h, p: (0, 0, h)),
            ]
            + [pl.BlockSpec((len(piece), 4, LANES), lambda h, p: (0, 0, h)) for piece in everyone],
            out_specs=pl.BlockSpec((length, LANES), col),
            scratch_shapes=[pltpu.VMEM((count, 4, LANES), jnp.float32)],
        ),
        out_shape=jax.ShapeDtypeStruct((length, channels), jnp.bfloat16),
        compiler_params=pltpu.CompilerParams(vmem_limit_bytes=60 << 20),
        name="carries",
    )(place, local, forward, backward, chunks, *everyone)


def prepare_kernel(
    ids_ref, in_ref, gain_ref, routes_ref, scores_ref, share_ref, *send_refs, block_rows, experts, capacity, cores
):
    f32, bf16 = jnp.float32, jnp.bfloat16
    rows = in_ref.shape[0]
    wide = in_ref[...].astype(f32)
    scale = lax.rsqrt(jnp.mean(wide * wide, axis=1, keepdims=True) + EPSILON)
    normed = (wide * scale * gain_ref[...]).astype(bf16)
    first, second = routes_ref[0:1, :], routes_ref[1:2, :]
    row = lax.broadcasted_iota(jnp.int32, (rows, rows), 0)
    col = lax.broadcasted_iota(jnp.int32, (rows, rows), 1)
    earlier = ((row // block_rows == col // block_rows) & (row < col)).astype(f32).astype(bf16)

    def placed(expert, place):
        named = ((first == expert) | (second == expert)).astype(f32)
        rank = jnp.dot(named.astype(bf16), earlier, preferred_element_type=f32)
        return jnp.where(rank == place.astype(f32), named, 0.0)

    slots = experts * capacity
    slot = lax.broadcasted_iota(jnp.int32, (slots, rows), 0)
    scores = scores_ref[...]
    shares = scores / jnp.sum(scores, axis=0, keepdims=True)
    held = placed(slot // capacity, slot % capacity) * jnp.where(
        first == slot // capacity, shares[0:1], shares[1:2]
    )
    high = held.astype(bf16)
    low = (held - high.astype(f32)).astype(bf16)
    row = lax.broadcasted_iota(jnp.int32, (block_rows, rows), 0)
    col = lax.broadcasted_iota(jnp.int32, (block_rows, rows), 1)
    own = (col == row + ids_ref[1] * block_rows).astype(f32).astype(bf16)
    for i, part in enumerate((high, low)):
        share_ref[i] = lax.dot_general(
            own, part, (((1,), (1,)), ((), ())), preferred_element_type=f32
        ).astype(bf16)

    blocks = rows // block_rows
    each = blocks * capacity
    width = each * experts // cores
    slot = lax.broadcasted_iota(jnp.int32, (width, rows), 0)
    token = lax.broadcasted_iota(jnp.int32, (width, rows), 1)
    planes = blocks // cores
    block = ((slot // capacity) % planes) * cores + (slot // (capacity * planes)) % cores
    distance = (slot // each + 1 + ids_ref[0] * (experts // cores)) % experts
    pick = placed(distance ^ ids_ref[2], slot % capacity)
    pick = jnp.where(token // block_rows == block, pick, 0.0).astype(bf16)
    send = jnp.dot(pick, normed, preferred_element_type=f32).astype(bf16)
    for d in range(experts // cores):
        send_refs[d][...] = send[d * each : (d + 1) * each]


def prepare(ids, expert_in, gain, routes, scores, block_rows, experts, capacity, cores):
    rows, model = expert_in.shape
    slots = experts * capacity
    each = rows // block_rows * capacity
    whole = lambda *shape: pl.BlockSpec(shape, lambda i, c: (0,) * len(shape))
    return pl.pallas_call(
        functools.partial(
            prepare_kernel, block_rows=block_rows, experts=experts, capacity=capacity, cores=cores
        ),
        grid_spec=pltpu.PrefetchScalarGridSpec(
            num_scalar_prefetch=1,
            grid=(1,),
            in_specs=[whole(rows, model), whole(1, model), whole(TOP_K, rows), whole(TOP_K, rows)],
            out_specs=[whole(2, block_rows, slots)] + [whole(each, model)] * (experts // cores),
        ),
        out_shape=[
            jax.ShapeDtypeStruct((2, block_rows, slots), jnp.bfloat16),
        ]
        + [jax.ShapeDtypeStruct((each, model), jnp.bfloat16)] * (experts // cores),
        compiler_params=pltpu.CompilerParams(vmem_limit_bytes=24 << 20),
        name="prepare",
    )(ids, far(expert_in), far(gain.reshape(1, model)), far(routes.T), far(scores.T))


def expert_kernel(groups, cores, ids_ref, own_ref, other_ref, gate_ref, up_ref, down_ref, keep_ref, send_ref, rows_ref, hidden_ref):
    f32, bf16 = jnp.float32, jnp.bfloat16
    half, model = own_ref.shape
    hidden = gate_ref.shape[1]
    wide, tall = math.gcd(hidden, 256), math.gcd(model, 256)
    core, place = ids_ref[0], ids_ref[2]
    count = groups // cores
    each = half // groups
    for s, ref in enumerate((own_ref, other_ref)):
        share = core if s == 0 else cores - 1 - core
        for k in range(count):
            to = lax.rem(k + 1 + share * count, groups) ^ place
            for t in range(cores):
                kind = core if t == 0 else cores - 1 - core
                src = pl.ds(pl.multiple_of((k * cores + kind) * each, each), each)
                dst = pl.ds(pl.multiple_of(t * half + to * each, each), each)
                rows_ref[dst, :] = ref[src, :]
    for f in range(0, hidden, wide):
        gate = jnp.dot(rows_ref[...], gate_ref[:, f : f + wide], preferred_element_type=f32)
        up = jnp.dot(rows_ref[...], up_ref[:, f : f + wide], preferred_element_type=f32)
        hidden_ref[:, f : f + wide] = (jax.nn.silu(gate) * up).astype(bf16)
    for n in range(0, model, tall):
        out = jnp.dot(hidden_ref[...], down_ref[:, n : n + tall], preferred_element_type=f32).astype(bf16)
        keep_ref[:, n : n + tall] = out[0:half]
        send_ref[:, n : n + tall] = out[half:]


def expert(ids, groups, cores, own, other, gate_weight, up_weight, down_weight):
    half, model = own.shape
    hidden = gate_weight.shape[1]
    bf16 = jnp.bfloat16
    vmem = pl.BlockSpec(memory_space=pltpu.VMEM)
    return pl.pallas_call(
        functools.partial(expert_kernel, groups, cores),
        in_specs=[pl.BlockSpec(memory_space=pltpu.SMEM)] + [vmem] * 5,
        out_specs=[vmem, vmem],
        out_shape=[jax.ShapeDtypeStruct((half, model), bf16)] * 2,
        scratch_shapes=[pltpu.VMEM((2 * half, model), bf16), pltpu.VMEM((2 * half, hidden), bf16)],
        compiler_params=pltpu.CompilerParams(vmem_limit_bytes=20 << 20),
        name="experts",
    )(ids, own, other, gate_weight, up_weight, down_weight)


def combine_kernel(back_ref, share_ref, out_ref):
    experts, parts, capacity, model = back_ref.shape
    total = None
    for p in range(parts):
        rows = back_ref[:, p].reshape(experts * capacity, model)
        for i in range(2):
            part = jnp.dot(share_ref[i], rows, preferred_element_type=jnp.float32)
            total = part if total is None else total + part
    out_ref[...] = total.astype(jnp.bfloat16)


def combine(back, share):
    model = back.shape[-1]
    return pl.pallas_call(
        combine_kernel,
        out_shape=jax.ShapeDtypeStruct((share.shape[1], model), jnp.bfloat16),
        compiler_params=pltpu.CompilerParams(vmem_limit_bytes=24 << 20),
        name="combine",
    )(back, share)


def local(
    x_path,
    gate_path,
    conv_taps,
    decay_gate_w,
    input_gate_w,
    decay_rate,
    decay_shift,
    expert_in,
    norm_gain,
    routes,
    route_scores,
    gate_weight,
    up_weight,
    down_weight,
):
    experts = lax.axis_size("ep")
    planes = lax.axis_size("plane")
    cores = lax.axis_size("core")
    place = lax.axis_index("ep")
    core = lax.axis_index("core")
    block = lax.axis_index("plane") * cores + core
    length = x_path.shape[0]
    group_rows, model = expert_in.shape
    block_rows = group_rows // (planes * cores)
    capacity = max(2, 2 * block_rows * TOP_K // experts)

    up = [(i, i + 1) for i in range(experts - 1)]
    down = [(j, i) for i, j in up]
    swap = [(i, cores - 1 - i) for i in range(cores)]
    far_by = lambda d: [(i, i ^ d) for i in range(experts)]
    ids = jnp.stack([core, block, place]).astype(jnp.int32)
    before = lax.ppermute(x_path[length - 2 :], "ep", up)
    after = lax.ppermute(x_path[:2], "ep", down)
    share, *outgoing = prepare(
        ids,
        expert_in,
        norm_gain,
        routes,
        route_scores,
        block_rows,
        experts,
        capacity,
        cores,
    )
    arrived = []
    for k, rows in enumerate(outgoing):
        away = [(k + 1 + c * len(outgoing)) % experts for c in range(cores)]
        pairs = [
            (i * cores + c, (i ^ away[c]) * cores + c) for i in range(experts) for c in range(cores)
        ]
        arrived.append(lax.ppermute(rows, ("ep", "core"), pairs))

    arrays = (
        x_path,
        gate_path,
        before,
        after,
        conv_taps,
        decay_gate_w,
        input_gate_w,
        decay_rate,
        decay_shift,
    )
    weights = (gate_weight, up_weight, down_weight)
    heads = decay_gate_w.shape[1]
    (mixed, forward, backward, chunks, totals), weights = local_recurrence(0, heads, arrays, weights, ())
    *arrived, totals = lax.optimization_barrier((*arrived, totals))
    arrived = jnp.concatenate(arrived, axis=0)
    other = lax.ppermute(arrived, "core", swap)
    everyone = [totals[None]]
    have = 1
    while have < experts:
        held = everyone[0] if have == 1 else jnp.concatenate(everyone, axis=0)
        everyone.append(lax.ppermute(held, "ep", far_by(have)))
        have *= 2
    keep, send = expert(ids, experts, cores, arrived, other, *weights)
    theirs = lax.ppermute(send, "core", swap)
    keep = (keep.astype(jnp.float32) + theirs.astype(jnp.float32)).astype(jnp.bfloat16)
    back = lax.all_to_all(
        keep.reshape(experts * planes, capacity, model), ("ep", "plane"), 0, 0, tiled=True
    ).reshape(experts, planes, capacity, model)
    recurrent_out = add_carries(
        place.reshape(1).astype(jnp.int32), mixed, forward, backward, chunks, everyone
    )
    expert_out = combine(back, share)
    return (recurrent_out, expert_out)


def solution(mesh):
    experts, tp = mesh.shape["ep"], mesh.shape["tp"]
    cores = 2
    fine = Mesh(mesh.devices.reshape(experts, tp // cores, cores), ("ep", "plane", "core"))
    tp = ("plane", "core")
    in_specs = (
        P("ep", tp),
        P("ep", tp),
        P(None, tp),
        P(None, tp, None, None),
        P(None, tp, None, None),
        P(None, tp),
        P("ep", tp),
        P("ep", None),
        P(),
        P("ep", None),
        P("ep", None),
        P("ep", None, tp),
        P("ep", None, tp),
        P("ep", tp, None),
    )
    out_specs = (P("ep", tp), P(("ep", "plane", "core"), None))
    return jax.shard_map(local, mesh=fine, in_specs=in_specs, out_specs=out_specs, check_vma=False)
```

profile of v0, /device:TPU:0, one launch (start us, length us, event | category | flops | bytes accessed | tf_op | source)
XLA Modules:
  0.0 72.3 jit_solution(10366744228178566693)
XLA Ops:
  0.6 0.1 pad_add_fusion.ids_ref
  0.7 2.1 %prepare.1 = (bf16[2,16,64]{2,1,0:T(8,128)(2,1)S(1)}, bf16[32,2048]{1,0:T(8,128)(2,1)S(1)}, bf16[32,2048]{1,0:T(8,128)(2,1)S(1)}, bf16[32,2048]{1,0:T(8,128)(2,1)S(1)}, bf16[32,2048]{1,0:T(8,128)(2,1)S(1)}) custom-call(s32[3]{0:T(128)S(1)} %pad_add_fusion.ids_ref, bf16[64,2048]{1,0:T(8,128)(2,1)} %in_ref.1, f32[1,2048]{1,0:T(1,128)} %bitcast.17, ...), custom_call_target="tpu_custom_call" | custom-call | tf_op jit(solution)/shard_map/prepare/pallas_call | solution.py:347
  2.8 3.0 %collective-permute-start.2 = (bf16[32,2048]{1,0:T(8,128)(2,1)S(1)}, bf16[32,2048]{1,0:T(8,128)(2,1)S(1)}, u32[]{:S(2)}, u32[]{:S(2)}) collective-permute-start(bf16[32,2048]{1,0:T(8,128)(2,1)S(1)} %get-tuple-element.26), channel_id=1, source_target_pairs={{0,4},{1,21},{4,0},{5,17},{8,12},{9,29},{12,8},{13,25},{16,20},{17... | collective-permute-start | bytes 393224 | tf_op jit(solution)/shard_map/ppermute | solution.py:481
  5.8 1.6 %collective-permute-start.3 = (bf16[32,2048]{1,0:T(8,128)(2,1)S(1)}, bf16[32,2048]{1,0:T(8,128)(2,1)S(1)}, u32[]{:S(2)}, u32[]{:S(2)}) collective-permute-start(bf16[32,2048]{1,0:T(8,128)(2,1)S(1)} %get-tuple-element.27), channel_id=1, source_target_pairs={{0,8},{1,25},{4,12},{5,29},{8,0},{9,17},{12,4},{13,21},{16,24},{17... | collective-permute-start | bytes 393224 | tf_op jit(solution)/shard_map/ppermute | solution.py:481
  7.4 0.0 collective-permute-start.4
  7.4 4.9 %collective-permute-start.5 = (bf16[32,2048]{1,0:T(8,128)(2,1)S(1)}, bf16[32,2048]{1,0:T(8,128)(2,1)S(1)}, u32[]{:S(2)}, u32[]{:S(2)}) collective-permute-start(bf16[32,2048]{1,0:T(8,128)(2,1)S(1)} %get-tuple-element.29), channel_id=1, source_target_pairs={{0,16},{1,1},{4,20},{5,5},{8,24},{9,9},{12,28},{13,13},{16,0},{17,... | collective-permute-start | bytes 393224 | tf_op jit(solution)/shard_map/ppermute | solution.py:481
  12.3 0.7 %fusion.1 = (bf16[2,512]{1,0:T(2,128)(2,1)S(1)}, bf16[2,512]{1,0:T(2,128)(2,1)S(1)}) fusion(bf16[1024,512]{1,0:T(8,128)(2,1)} %refs_0_.1), kind=kLoop, calls=%fused_computation.9 | loop fusion | bytes 8192 | tf_op jit(solution)/shard_map/slice | solution.py:463
  13.0 1.3 %collective-permute-start.1 = (bf16[2,512]{1,0:T(2,128)(2,1)S(1)}, bf16[2,512]{1,0:T(2,128)(2,1)S(1)}, u32[]{:S(2)}, u32[]{:S(2)}) collective-permute-start(bf16[2,512]{1,0:T(2,128)(2,1)S(1)} %get-tuple-element.42), channel_id=1, source_target_pairs={{4,0},{8,4},{12,8},{16,12},{20,16},{24,20},{28,24},{5,1},{9,5},{13... | collective-permute-start | bytes 6152 | tf_op jit(solution)/shard_map/ppermute | solution.py:463
  14.3 4.2 %collective-permute-done.1.refs_3_ = bf16[2,512]{1,0:T(2,128)(2,1)S(1)} collective-permute-done((bf16[2,512]{1,0:T(2,128)(2,1)S(1)}, bf16[2,512]{1,0:T(2,128)(2,1)S(1)}, u32[]{:S(2)}, u32[]{:S(2)}) %collective-permute-start.1) | collective-permute-done | bytes 2080 | tf_op jit(solution)/shard_map/ppermute | solution.py:463
  18.5 4.3 %collective-permute-start = (bf16[2,512]{1,0:T(2,128)(2,1)S(1)}, bf16[2,512]{1,0:T(2,128)(2,1)S(1)}, u32[]{:S(2)}, u32[]{:S(2)}) collective-permute-start(bf16[2,512]{1,0:T(2,128)(2,1)S(1)} %get-tuple-element.43), channel_id=1, source_target_pairs={{0,4},{4,8},{8,12},{12,16},{16,20},{20,24},{24,28},{1,5},{5,9},{9,... | collective-permute-start | bytes 6152 | tf_op jit(solution)/shard_map/ppermute | solution.py:462
  22.8 1.3 %collective-permute-done.refs_2_ = bf16[2,512]{1,0:T(2,128)(2,1)S(1)} collective-permute-done((bf16[2,512]{1,0:T(2,128)(2,1)S(1)}, bf16[2,512]{1,0:T(2,128)(2,1)S(1)}, u32[]{:S(2)}, u32[]{:S(2)}) %collective-permute-start) | collective-permute-done | bytes 2080 | tf_op jit(solution)/shard_map/ppermute | solution.py:462
  24.1 11.7 %recurrence.1 = (bf16[1024,512]{1,0:T(8,128)(2,1)}, bf16[1024,512]{1,0:T(8,128)(2,1)}, bf16[1024,512]{1,0:T(8,128)(2,1)}, f32[4,8,512]{2,1,0:T(8,128)}, f32[4,51...) custom-call(bf16[1024,512]{1,0:T(8,128)(2,1)} %refs_0_.1, ...), custom_call_target="tpu_custom_call" | custom-call | tf_op jit(solution)/shard_map/recurrence/pallas_call | solution.py:183
  35.8 0.0 collective-permute-done.2
  35.9 0.0 collective-permute-done.4
  35.9 0.0 collective-permute-done.5
  36.0 0.1 collective-permute-start.9
  36.0 1.9 %collective-permute-done.9.other_ref = bf16[128,2048]{1,0:T(8,128)(2,1)S(1)} collective-permute-done((bf16[128,2048]{1,0:T(8,128)(2,1)S(1)}, bf16[128,2048]{1,0:T(8,128)(2,1)S(1)}, u32[]{:S(2)}, u32[]{:S(2)}) %collective-permute-start.9) | collective-permute-done | bytes 524320 | tf_op jit(solution)/shard_map/ppermute | solution.py:499
  37.9 4.1 %experts.1 = (bf16[128,2048]{1,0:T(8,128)(2,1)S(1)}, bf16[128,2048]{1,0:T(8,128)(2,1)S(1)}) custom-call(s32[3]{0:T(128)S(1)} %pad_add_fusion.ids_ref, bf16[128,2048]{1,0:T(8,128)(2,1)S(1)} %constant_dynamic-update-slice_fusion.own_ref, bf16[128,2048]{1,0:T(8,128)(2,1)S(1)} %collective-permute-done.9.other_ref, ...), custom_call_target="tpu_custom_call" | custom-call | tf_op jit(solution)/shard_map/experts/pallas_call | solution.py:398
  42.1 0.2 collective-permute-start.10
  42.3 1.8 %collective-permute-done.10 = bf16[128,2048]{1,0:T(8,128)(2,1)S(1)} collective-permute-done((bf16[128,2048]{1,0:T(8,128)(2,1)S(1)}, bf16[128,2048]{1,0:T(8,128)(2,1)S(1)}, u32[]{:S(2)}, u32[]{:S(2)}) %collective-permute-start.10) | collective-permute-done | bytes 524320 | tf_op jit(solution)/shard_map/ppermute | solution.py:507
  44.1 0.9 %fusion = bf16[16,8,2048]{2,1,0:T(8,128)(2,1)} fusion(bf16[128,2048]{1,0:T(8,128)(2,1)S(1)} %collective-permute-done.10, bf16[128,2048]{1,0:T(8,128)(2,1)S(1)} %get-tuple-element.39), kind=kLoop, calls=%fused_computation.1 | loop fusion | flops 1048576 | bytes 1572864 | tf_op jit(solution)/shard_map/reshape | solution.py:510
  45.0 5.6 %all-to-all-start = ((bf16[16,8,2048]{2,1,0:T(8,128)(2,1)}), bf16[16,8,2048]{2,1,0:T(8,128)(2,1)S(1)}, u32[]{:S(2)}, u32[]{:S(2)}) async-start(bf16[16,8,2048]{2,1,0:T(8,128)(2,1)} %fusion), calls=%async_computation | async-start | bytes 1048576 | tf_op jit(solution)/shard_map/all_to_all | solution.py:509
  50.6 2.0 %collective-permute-start.6 = (f32[1,4,512]{2,1,0:T(4,128)S(1)}, f32[1,4,512]{2,1,0:T(4,128)S(1)}, u32[]{:S(2)}, u32[]{:S(2)}) collective-permute-start(f32[1,4,512]{2,1,0:T(4,128)S(1)} %bitcast.13), channel_id=1, source_target_pairs={{0,4},{4,0},{8,12},{12,8},{16,20},{20,16},{24,28},{28,24},{1,5},{5... | collective-permute-start | bytes 24584 | tf_op jit(solution)/shard_map/ppermute | solution.py:504
  52.6 3.4 %collective-permute-done.6.refs_1_ = f32[1,4,512]{2,1,0:T(4,128)S(1)} collective-permute-done((f32[1,4,512]{2,1,0:T(4,128)S(1)}, f32[1,4,512]{2,1,0:T(4,128)S(1)}, u32[]{:S(2)}, u32[]{:S(2)}) %collective-permute-start.6) | collective-permute-done | bytes 8224 | tf_op jit(solution)/shard_map/ppermute | solution.py:504
  56.0 0.9 %collective-permute-start.7 = (f32[2,4,512]{2,1,0:T(4,128)S(1)}, f32[2,4,512]{2,1,0:T(4,128)S(1)}, u32[]{:S(2)}, u32[]{:S(2)}) collective-permute-start(f32[2,4,512]{2,1,0:T(4,128)S(1)} %pad_maximum_fusion.1), channel_id=1, source_target_pairs={{0,8},{4,12},{8,0},{12,4},{16,24},{20,28},{24,16},{28,20},{1,9},{5... | collective-permute-start | bytes 49160 | tf_op jit(solution)/shard_map/ppermute | solution.py:504
  56.9 3.1 %collective-permute-done.7.refs_2_ = f32[2,4,512]{2,1,0:T(4,128)S(1)} collective-permute-done((f32[2,4,512]{2,1,0:T(4,128)S(1)}, f32[2,4,512]{2,1,0:T(4,128)S(1)}, u32[]{:S(2)}, u32[]{:S(2)}) %collective-permute-start.7) | collective-permute-done | bytes 16416 | tf_op jit(solution)/shard_map/ppermute | solution.py:504
  60.0 4.4 %collective-permute-start.8 = (f32[4,4,512]{2,1,0:T(4,128)S(1)}, f32[4,4,512]{2,1,0:T(4,128)S(1)}, u32[]{:S(2)}, u32[]{:S(2)}) collective-permute-start(f32[4,4,512]{2,1,0:T(4,128)S(1)} %pad_maximum_fusion), channel_id=1, source_target_pairs={{0,16},{4,20},{8,24},{12,28},{16,0},{20,4},{24,8},{28,12},{1,17},{... | collective-permute-start | bytes 98312 | tf_op jit(solution)/shard_map/ppermute | solution.py:504
  64.4 2.3 %collective-permute-done.8.refs_3_ = f32[4,4,512]{2,1,0:T(4,128)S(1)} collective-permute-done((f32[4,4,512]{2,1,0:T(4,128)S(1)}, f32[4,4,512]{2,1,0:T(4,128)S(1)}, u32[]{:S(2)}, u32[]{:S(2)}) %collective-permute-start.8) | collective-permute-done | bytes 32800 | tf_op jit(solution)/shard_map/ppermute | solution.py:504
  66.7 0.6 copy-done.3
  67.3 4.1 %carries.1 = bf16[1024,512]{1,0:T(8,128)(2,1)} custom-call(s32[1]{0:T(128)} %bitcast.place_ref, bf16[1024,512]{1,0:T(8,128)(2,1)} %get-tuple-element.22.local_ref, bf16[1024,512]{1,0:T(8,128)(2,1)} %get-tuple-element.23.forward_ref, bf16[1024,512]{1,0:T(8,128)(2,1)} %get-tuple-element.24.backward_ref, f32[4,8,512]{2,1,0:T(8,128)} %get-tuple-element.25.chunk_ref, ...), custom_call_target="tpu_custom_call" | custom-call | tf_op jit(solution)/shard_map/carries/pallas_call | solution.py:271
  71.4 0.0 all-to-all-done
  71.4 0.9 %combine.1 = bf16[16,2048]{1,0:T(8,128)(2,1)} custom-call(bf16[8,2,8,2048]{3,2,1,0:T(8,128)(2,1)S(1)} %bitcast.11, bf16[2,16,64]{2,1,0:T(8,128)(2,1)S(1)} %get-tuple-element.41.share_ref), custom_call_target="tpu_custom_call" | custom-call | tf_op jit(solution)/shard_map/combine/pallas_call | solution.py:422
  (14 shorter events, 0.1 us)
Async XLA Ops:
  2.8 33.1 %collective-permute-start.2 = (bf16[32,2048]{1,0:T(8,128)(2,1)S(1)}, bf16[32,2048]{1,0:T(8,128)(2,1)S(1)}, u32[]{:S(2)}, u32[]{:S(2)}) collective-permute-start(bf16[32,2048]{1,0:T(8,128)(2,1)S(1)} %get-tuple-element.26), channel_id=1, source_target_pairs={{0,4},{1,21},{4,0},{5,17},{8,12},{9,29},{12,8},{13,25},{16,20},{17... | collective-permute-start | bytes 393224 | tf_op jit(solution)/shard_map/ppermute | solution.py:481
  5.8 30.1 %collective-permute-start.3 = (bf16[32,2048]{1,0:T(8,128)(2,1)S(1)}, bf16[32,2048]{1,0:T(8,128)(2,1)S(1)}, u32[]{:S(2)}, u32[]{:S(2)}) collective-permute-start(bf16[32,2048]{1,0:T(8,128)(2,1)S(1)} %get-tuple-element.27), channel_id=1, source_target_pairs={{0,8},{1,25},{4,12},{5,29},{8,0},{9,17},{12,4},{13,21},{16,24},{17... | collective-permute-start | bytes 393224 | tf_op jit(solution)/shard_map/ppermute | solution.py:481
  7.4 28.5 %collective-permute-start.4 = (bf16[32,2048]{1,0:T(8,128)(2,1)S(1)}, bf16[32,2048]{1,0:T(8,128)(2,1)S(1)}, u32[]{:S(2)}, u32[]{:S(2)}) collective-permute-start(bf16[32,2048]{1,0:T(8,128)(2,1)S(1)} %get-tuple-element.28), channel_id=1, source_target_pairs={{0,12},{1,29},{4,8},{5,25},{8,4},{9,21},{12,0},{13,17},{16,28},{17... | collective-permute-start | bytes 393224 | tf_op jit(solution)/shard_map/ppermute | solution.py:481
  7.4 28.5 %collective-permute-start.5 = (bf16[32,2048]{1,0:T(8,128)(2,1)S(1)}, bf16[32,2048]{1,0:T(8,128)(2,1)S(1)}, u32[]{:S(2)}, u32[]{:S(2)}) collective-permute-start(bf16[32,2048]{1,0:T(8,128)(2,1)S(1)} %get-tuple-element.29), channel_id=1, source_target_pairs={{0,16},{1,1},{4,20},{5,5},{8,24},{9,9},{12,28},{13,13},{16,0},{17,... | collective-permute-start | bytes 393224 | tf_op jit(solution)/shard_map/ppermute | solution.py:481
  13.0 5.5 %collective-permute-start.1 = (bf16[2,512]{1,0:T(2,128)(2,1)S(1)}, bf16[2,512]{1,0:T(2,128)(2,1)S(1)}, u32[]{:S(2)}, u32[]{:S(2)}) collective-permute-start(bf16[2,512]{1,0:T(2,128)(2,1)S(1)} %get-tuple-element.42), channel_id=1, source_target_pairs={{4,0},{8,4},{12,8},{16,12},{20,16},{24,20},{28,24},{5,1},{9,5},{13... | collective-permute-start | bytes 6152 | tf_op jit(solution)/shard_map/ppermute | solution.py:463
  18.5 5.6 %collective-permute-start = (bf16[2,512]{1,0:T(2,128)(2,1)S(1)}, bf16[2,512]{1,0:T(2,128)(2,1)S(1)}, u32[]{:S(2)}, u32[]{:S(2)}) collective-permute-start(bf16[2,512]{1,0:T(2,128)(2,1)S(1)} %get-tuple-element.43), channel_id=1, source_target_pairs={{0,4},{4,8},{8,12},{12,16},{16,20},{20,24},{24,28},{1,5},{5,9},{9,... | collective-permute-start | bytes 6152 | tf_op jit(solution)/shard_map/ppermute | solution.py:462
  36.0 2.0 %collective-permute-start.9 = (bf16[128,2048]{1,0:T(8,128)(2,1)S(1)}, bf16[128,2048]{1,0:T(8,128)(2,1)S(1)}, u32[]{:S(2)}, u32[]{:S(2)}) collective-permute-start(bf16[128,2048]{1,0:T(8,128)(2,1)S(1)} %constant_dynamic-update-slice_fusion.own_ref), channel_id=1, source_target_pairs={{0,1},{1,0},{2,3},{3,2},{4,5},{5,4},{6,7},{7,6},{8,9},{9,8},{10,11... | collective-permute-start | bytes 1572872 | tf_op jit(solution)/shard_map/ppermute | solution.py:499
  37.9 12.7 %copy-start = (f32[4,512]{1,0:T(4,128)S(1)}, f32[4,512]{1,0:T(4,128)}, u32[]{:S(2)}) copy-start(f32[4,512]{1,0:T(4,128)} %get-tuple-element.31) | copy-start | bytes 24580
  42.1 2.0 %collective-permute-start.10 = (bf16[128,2048]{1,0:T(8,128)(2,1)S(1)}, bf16[128,2048]{1,0:T(8,128)(2,1)S(1)}, u32[]{:S(2)}, u32[]{:S(2)}) collective-permute-start(bf16[128,2048]{1,0:T(8,128)(2,1)S(1)} %get-tuple-element.40), channel_id=1, source_target_pairs={{0,1},{1,0},{2,3},{3,2},{4,5},{5,4},{6,7},{7,6},{8,9},{9,8},{10,11... | collective-permute-start | bytes 1572872 | tf_op jit(solution)/shard_map/ppermute | solution.py:507
  45.0 26.4 %all-to-all-start = ((bf16[16,8,2048]{2,1,0:T(8,128)(2,1)}), bf16[16,8,2048]{2,1,0:T(8,128)(2,1)S(1)}, u32[]{:S(2)}, u32[]{:S(2)}) async-start(bf16[16,8,2048]{2,1,0:T(8,128)(2,1)} %fusion), calls=%async_computation | async-start | bytes 1048576 | tf_op jit(solution)/shard_map/all_to_all | solution.py:509
  50.6 5.4 %collective-permute-start.6 = (f32[1,4,512]{2,1,0:T(4,128)S(1)}, f32[1,4,512]{2,1,0:T(4,128)S(1)}, u32[]{:S(2)}, u32[]{:S(2)}) collective-permute-start(f32[1,4,512]{2,1,0:T(4,128)S(1)} %bitcast.13), channel_id=1, source_target_pairs={{0,4},{4,0},{8,12},{12,8},{16,20},{20,16},{24,28},{28,24},{1,5},{5... | collective-permute-start | bytes 24584 | tf_op jit(solution)/shard_map/ppermute | solution.py:504
  56.0 10.7 %copy-start.1 = (f32[1,4,512]{2,1,0:T(4,128)}, f32[1,4,512]{2,1,0:T(4,128)S(1)}, u32[]{:S(2)}) copy-start(f32[1,4,512]{2,1,0:T(4,128)S(1)} %collective-permute-done.6.refs_1_) | copy-start | bytes 24580
  56.0 4.0 %collective-permute-start.7 = (f32[2,4,512]{2,1,0:T(4,128)S(1)}, f32[2,4,512]{2,1,0:T(4,128)S(1)}, u32[]{:S(2)}, u32[]{:S(2)}) collective-permute-start(f32[2,4,512]{2,1,0:T(4,128)S(1)} %pad_maximum_fusion.1), channel_id=1, source_target_pairs={{0,8},{4,12},{8,0},{12,4},{16,24},{20,28},{24,16},{28,20},{1,9},{5... | collective-permute-start | bytes 49160 | tf_op jit(solution)/shard_map/ppermute | solution.py:504
  60.0 6.7 %copy-start.2 = (f32[2,4,512]{2,1,0:T(4,128)}, f32[2,4,512]{2,1,0:T(4,128)S(1)}, u32[]{:S(2)}) copy-start(f32[2,4,512]{2,1,0:T(4,128)S(1)} %collective-permute-done.7.refs_2_) | copy-start | bytes 49156
  60.0 6.7 %collective-permute-start.8 = (f32[4,4,512]{2,1,0:T(4,128)S(1)}, f32[4,4,512]{2,1,0:T(4,128)S(1)}, u32[]{:S(2)}, u32[]{:S(2)}) collective-permute-start(f32[4,4,512]{2,1,0:T(4,128)S(1)} %pad_maximum_fusion), channel_id=1, source_target_pairs={{0,16},{4,20},{8,24},{12,28},{16,0},{20,4},{24,8},{28,12},{1,17},{... | collective-permute-start | bytes 98312 | tf_op jit(solution)/shard_map/ppermute | solution.py:504
  66.7 0.6 copy-start.3
where the time goes:
time: 72.7 us; the launch traced here: 72.3 us
  starting transfers between devices  28.3 us (39%)
  Pallas kernels  22.9 us (31%)
  waiting for transfers between devices  17.9 us (25%)
  local copies, waits for them, and re-layouts  1.38 us (2%)
  other arithmetic  1.01 us (1%)
  between operations  0.79 us (1%)
    pallas_call x1, Pallas kernels, local_recurrence(): pl.pallas_call(functools.partial(gates_kernel, first, len(weights), len(p...  11.7 us
    ppermute x4, starting transfers between devices, local(): arrived.append(lax.ppermute(rows, ('ep', 'core'), pairs))  9.51 us
    ppermute x3, waiting for transfers between devices, local(): everyone.append(lax.ppermute(held, 'ep', far_by(have)))  8.76 us
    ppermute x3, starting transfers between devices, local(): everyone.append(lax.ppermute(held, 'ep', far_by(have)))  7.3 us
    all_to_all x1, starting transfers between devices, local(): lax.all_to_all(keep.reshape(experts * planes, capacity, model), ('ep', 'p...  5.62 us
    ppermute x1, starting transfers between devices, local(): before = lax.ppermute(x_path[length - 2:], 'ep', up)  4.3 us
    ppermute x1, waiting for transfers between devices, local(): after = lax.ppermute(x_path[:2], 'ep', down)  4.18 us
    pallas_call x1, Pallas kernels, expert(): pl.pallas_call(functools.partial(expert_kernel, groups, cores), in_specs=...  4.12 us
  transfers between devices with their start and end apart: 12, of which 7 were waited for; matrix products, arithmetic and copies ran while one was open for 1% of the time, Pallas kernels for 22%

commit v1 on v0

--- a/solution.py
+++ b/solution.py
@@ -13,7 +13,7 @@
 EPSILON = 1e-06
 LANES = 128
 CHUNKS = 8
-STEPS = 32
+STEPS = 64
 LOG2E = math.log2(math.e)
 LN2 = math.log(2.0)
 SERIES = (-2.0 * LN2, -((2.0 * LN2) ** 2) / 2.0, -((2.0 * LN2) ** 3) / 6.0)
@@ -23,30 +23,37 @@
     return pltpu.with_memory_space_constraint(x, pltpu.HBM)
 
 
-def gates_kernel(first, fetched, filled, *refs):
-    x_ref, gate_ref, before_ref, after_ref, taps_ref, decay_w_ref, input_w_ref, rate_ref, shift_ref = refs[:9]
-    at = 9
+def gates_kernel(first, count, fetched, filled, *refs):
+    x_ref, before_ref, after_ref, taps_ref, decay_w_ref, input_w_ref, rate_ref, shift_ref = refs[:8]
+    at = 8
     sources = refs[at : at + fetched]
     at += fetched + filled
     local_ref, forward_ref, backward_ref, chunk_ref, total_ref = refs[at : at + 5]
     at += 5
     targets = refs[at : at + fetched]
     at += fetched
-    rows_ref, decay_ref, drive_ref, state_ref, prod_ref, sems = refs[at:]
+    rows_ref, decay_ref, drive_ref, state_ref, sems = refs[at:]
     length = x_ref.shape[0]
     per = length // CHUNKS
     pitch = per + 4
     f32 = jnp.float32
 
-    fetches = [
-        pltpu.make_async_copy(a.at[0], b, sems.at[i])
-        for i, (a, b) in enumerate(zip(sources, targets))
-    ]
-
-    @pl.when(pl.program_id(0) == 0)
-    def _():
-        for fetch in fetches:
-            fetch.start()
+    step = pl.program_id(0)
+
+    def fetch(h):
+        copies = []
+        for i, (a, b) in enumerate(zip(sources, targets)):
+            part = b.shape[0] // count
+            at = pl.ds(h * part, part)
+            copies.append(pltpu.make_async_copy(a.at[0, at], b.at[at], sems.at[i, h]))
+        return copies
+
+    for h in range(count):
+
+        @pl.when(step == h)
+        def _():
+            for copy in fetch(h):
+                copy.start()
 
     for s in range(CHUNKS):
         block = x_ref[s * per : (s + 1) * per, :].astype(f32)
@@ -101,11 +108,11 @@
                 for i in range(STEPS):
                     step = decay[i * CHUNKS : (i + 1) * CHUNKS]
                     state = step * state + drive[i * CHUNKS : (i + 1) * CHUNKS]
-                    prod = step * prod
-                    at = pl.ds(start + i * CHUNKS, CHUNKS)
-                    state_ref[at, :] = state
-                    row = pl.ds(base + i, CHUNKS, stride=pitch)
-                    prod_ref[0, row, :] = prod
+                    state_ref[pl.ds(start + i * CHUNKS, CHUNKS), :] = state
+                    held, prod = prod, step * prod
+                    if i % 2:
+                        two = pl.ds(start + (i - 1) * CHUNKS, 2 * CHUNKS)
+                        forward_ref[two, :] = jnp.concatenate([held, prod]).astype(forward_ref.dtype)
             else:
                 decay_ref[pl.ds(start, size), :] = decay
                 drive_ref[pl.ds(start, size), :] = drive
@@ -125,9 +132,13 @@
             step = decay_ref[at, :]
             state = step * state + drive_ref[at, :]
             prod = step * prod
-            row = pl.ds(base + i, CHUNKS, stride=pitch)
-            rows_ref[row, :] = state + state_ref[at, :]
-            prod_ref[1, row, :] = prod
+            total = state + state_ref[at, :]
+            if i % 2:
+                last_total, last_prod = total, prod
+            else:
+                two = pl.ds(start + i * CHUNKS, 2 * CHUNKS)
+                local_ref[two, :] = jnp.concatenate([total, last_total]).astype(local_ref.dtype)
+                backward_ref[two, :] = jnp.concatenate([prod, last_prod]).astype(backward_ref.dtype)
         return state, prod
 
     backward_end, backward_prod = lax.fori_loop(0, blocks, back, (zero, one))
@@ -149,30 +160,15 @@
     total_ref[2:3, :] = prod
     total_ref[3:4, :] = state
 
-    span = 64
-
-    def finish(b, none):
-        s = b // (per // span)
-        inner = (b % (per // span)) * span
-        nat = pl.ds(pl.multiple_of(b * span, span), span)
-        row = pl.ds(s * pitch + inner, span)
-        g = gate_ref[nat, :].astype(f32)
-        gelu = 0.5 * g * (1.0 + jnp.tanh(math.sqrt(2.0 / math.pi) * (g + 0.044715 * (g * g * g))))
-        local_ref[nat, :] = (rows_ref[row, :] * gelu).astype(local_ref.dtype)
-        forward_ref[nat, :] = (prod_ref[0, row, :] * gelu).astype(forward_ref.dtype)
-        backward_ref[nat, :] = (prod_ref[1, row, :] * gelu).astype(backward_ref.dtype)
-        return none
-
-    lax.fori_loop(0, length // span, finish, 0)
-
     @pl.when(pl.program_id(0) == pl.num_programs(0) - 1)
     def _():
-        for fetch in fetches:
-            fetch.wait()
+        for h in range(count):
+            for copy in fetch(h):
+                copy.wait()
 
 
 def local_recurrence(first, count, arrays, weights, partial):
-    x, gate, before, after, taps, decay_w, input_w, rate, shift = arrays
+    x, before, after, taps, decay_w, input_w, rate, shift = arrays
     length, channels = x.shape
     heads = decay_w.shape[1]
     per = length // CHUNKS
@@ -181,10 +177,9 @@
     bf16, f32 = jnp.bfloat16, jnp.float32
     any_ref = pl.BlockSpec(memory_space=pltpu.HBM)
     outs = pl.pallas_call(
-        functools.partial(gates_kernel, first, len(weights), len(partial)),
+        functools.partial(gates_kernel, first, count, len(weights), len(partial)),
         grid=(count,),
         in_specs=[
-            pl.BlockSpec((length, LANES), col),
             pl.BlockSpec((length, LANES), col),
             pl.BlockSpec((2, LANES), col),
             pl.BlockSpec((2, LANES), col),
@@ -216,55 +211,78 @@
             pltpu.VMEM((length, LANES), f32),
             pltpu.VMEM((length, LANES), f32),
             pltpu.VMEM((length, LANES), f32),
-            pltpu.VMEM((2, CHUNKS * pitch, LANES), f32),
-            pltpu.SemaphoreType.DMA((3,)),
+            pltpu.SemaphoreType.DMA((3, count)),
         ],
-        input_output_aliases={9 + len(weights) + i: i for i in range(len(partial))},
+        input_output_aliases={8 + len(weights) + i: i for i in range(len(partial))},
         compiler_params=pltpu.CompilerParams(vmem_limit_bytes=20 << 20),
         name="recurrence",
     )(
-        far(x), far(gate), before, after, far(taps), far(decay_w), far(input_w), far(rate), far(shift.T),
+        far(x), before, after, far(taps), far(decay_w), far(input_w), far(rate), far(shift.T),
         *map(far, weights), *map(far, partial)
     )
     return list(outs[:5]), list(outs[5:])
 
 
-def carry_kernel(place_ref, local_ref, forward_ref, backward_ref, chunk_ref, *refs):
-    *pieces, out_ref, all_ref = refs
+def carry_kernel(place_ref, gate_ref, local_ref, forward_ref, backward_ref, chunk_ref, *refs):
+    *pieces, out_ref, all_ref, ends_ref, rows_ref = refs
     length = local_ref.shape[0]
     per = length // CHUNKS
+    pitch = per + 4
     f32 = jnp.float32
     place = place_ref[0]
-    count = 0
-    for piece in pieces:
-        all_ref[count : count + piece.shape[0]] = piece[...]
-        count += piece.shape[0]
+    count = all_ref.shape[0]
+    away, bit = [0], count // 2
+    all_ref[0] = pieces[0][0]
+    for piece in pieces[1:]:
+        for i, d in enumerate(away):
+            all_ref[d ^ bit] = piece[i]
+        away += [d ^ bit for d in away]
+        bit //= 2
     carry = jnp.zeros((1, LANES), f32)
     for e in range(count):
         after = all_ref[e ^ place, 0:1] * carry + all_ref[e ^ place, 1:2]
         carry = jnp.where(e < place, after, carry)
-    ahead = [None] * CHUNKS
     for s in range(CHUNKS):
-        ahead[s] = carry
+        ends_ref[0, s : s + 1, :] = carry
         carry = chunk_ref[0, s : s + 1] * carry + chunk_ref[1, s : s + 1]
     carry = jnp.zeros((1, LANES), f32)
     for e in reversed(range(count)):
         after = all_ref[e ^ place, 2:3] * carry + all_ref[e ^ place, 3:4]
         carry = jnp.where(e > place, after, carry)
-    behind = [None] * CHUNKS
     for s in reversed(range(CHUNKS)):
-        behind[s] = carry
+        ends_ref[1, s : s + 1, :] = carry
         carry = chunk_ref[2, s : s + 1] * carry + chunk_ref[3, s : s + 1]
-    for s in range(CHUNKS):
-        at = slice(s * per, (s + 1) * per)
-        out_ref[at, :] = (
-            local_ref[at, :].astype(f32)
-            + forward_ref[at, :].astype(f32) * ahead[s]
-            + backward_ref[at, :].astype(f32) * behind[s]
-        ).astype(out_ref.dtype)
-
-
-def add_carries(place, local, forward, backward, chunks, everyone):
+    ahead, behind = ends_ref[0], ends_ref[1]
+    size = STEPS * CHUNKS
+
+    def add(b, none):
+        at = pl.ds(pl.multiple_of(b * size, size), size)
+        mixed = local_ref[at, :].astype(f32)
+        one = forward_ref[at, :].astype(f32)
+        two = backward_ref[at, :].astype(f32)
+        for i in range(STEPS):
+            v = slice(i * CHUNKS, (i + 1) * CHUNKS)
+            row = pl.ds(b * STEPS + i, CHUNKS, stride=pitch)
+            rows_ref[row, :] = mixed[v] + one[v] * ahead + two[v] * behind
+        return none
+
+    lax.fori_loop(0, per // STEPS, add, 0)
+    span = 64
+
+    def finish(b, none):
+        s = b // (per // span)
+        inner = (b % (per // span)) * span
+        nat = pl.ds(pl.multiple_of(b * span, span), span)
+        row = pl.ds(s * pitch + inner, span)
+        g = gate_ref[nat, :].astype(f32)
+        gelu = 0.5 * g * (1.0 + jnp.tanh(math.sqrt(2.0 / math.pi) * (g + 0.044715 * (g * g * g))))
+        out_ref[nat, :] = (rows_ref[row, :] * gelu).astype(out_ref.dtype)
+        return none
+
+    lax.fori_loop(0, length // span, finish, 0)
+
+
+def add_carries(place, gate, local, forward, backward, chunks, everyone):
     length, channels = local.shape
     count = sum(piece.shape[0] for piece in everyone)
     col = lambda h, p: (0, h)
@@ -273,20 +291,20 @@
         grid_spec=pltpu.PrefetchScalarGridSpec(
             num_scalar_prefetch=1,
             grid=(channels // LANES,),
-            in_specs=[
-                pl.BlockSpec((length, LANES), col),
-                pl.BlockSpec((length, LANES), col),
-                pl.BlockSpec((length, LANES), col),
-                pl.BlockSpec((4, CHUNKS, LANES), lambda h, p: (0, 0, h)),
-            ]
+            in_specs=[pl.BlockSpec((length, LANES), col)] * 4
+            + [pl.BlockSpec((4, CHUNKS, LANES), lambda h, p: (0, 0, h))]
             + [pl.BlockSpec((len(piece), 4, LANES), lambda h, p: (0, 0, h)) for piece in everyone],
             out_specs=pl.BlockSpec((length, LANES), col),
-            scratch_shapes=[pltpu.VMEM((count, 4, LANES), jnp.float32)],
+            scratch_shapes=[
+                pltpu.VMEM((count, 4, LANES), jnp.float32),
+                pltpu.VMEM((2, CHUNKS, LANES), jnp.float32),
+                pltpu.VMEM((length + 4 * CHUNKS, LANES), jnp.float32),
+            ],
         ),
         out_shape=jax.ShapeDtypeStruct((length, channels), jnp.bfloat16),
-        compiler_params=pltpu.CompilerParams(vmem_limit_bytes=60 << 20),
+        compiler_params=pltpu.CompilerParams(vmem_limit_bytes=20 << 20),
         name="carries",
-    )(place, local, forward, backward, chunks, *everyone)
+    )(place, far(gate), far(local), far(forward), far(backward), chunks, *everyone)
 
 
 def prepare_kernel(
@@ -482,7 +500,6 @@
 
     arrays = (
         x_path,
-        gate_path,
         before,
         after,
         conv_taps,
@@ -498,11 +515,11 @@
     arrived = jnp.concatenate(arrived, axis=0)
     other = lax.ppermute(arrived, "core", swap)
     everyone = [totals[None]]
-    have = 1
-    while have < experts:
-        held = everyone[0] if have == 1 else jnp.concatenate(everyone, axis=0)
-        everyone.append(lax.ppermute(held, "ep", far_by(have)))
-        have *= 2
+    bit = experts // 2
+    while bit:
+        held = everyone[0] if len(everyone) == 1 else jnp.concatenate(everyone, axis=0)
+        everyone.append(lax.ppermute(held, "ep", far_by(bit)))
+        bit //= 2
     keep, send = expert(ids, experts, cores, arrived, other, *weights)
     theirs = lax.ppermute(send, "core", swap)
     keep = (keep.astype(jnp.float32) + theirs.astype(jnp.float32)).astype(jnp.bfloat16)
@@ -510,7 +527,7 @@
         keep.reshape(experts * planes, capacity, model), ("ep", "plane"), 0, 0, tiled=True
     ).reshape(experts, planes, capacity, model)
     recurrent_out = add_carries(
-        place.reshape(1).astype(jnp.int32), mixed, forward, backward, chunks, everyone
+        place.reshape(1).astype(jnp.int32), gate_path, mixed, forward, backward, chunks, everyone
     )
     expert_out = combine(back, share)
     return (recurrent_out, expert_out)

time: 72.7 us -> 77.2 us (1.062)
  waiting for transfers between devices: 17.9 us -> 27.5 us
  starting transfers between devices: 28.3 us -> 25.4 us
  Pallas kernels: 22.9 us -> 21.3 us
    ppermute x3, waiting for transfers between devices: 8.76 us -> 18.3 us  [local(): everyone.append(lax.ppermute(held, 'ep', far_by(bit)))]
    ppermute x3, starting transfers between devices: 7.3 us -> 4.42 us  [local(): everyone.append(lax.ppermute(held, 'ep', far_by(bit)))]
    pallas_call x1, Pallas kernels: 11.7 us -> 9.17 us  [local_recurrence(): pl.pallas_call(functools.partial(gates_kernel, first, count, len(weights)...]
    pallas_call x1, Pallas kernels: 4.1 us -> 5.07 us  [add_carries(): pl.pallas_call(carry_kernel, grid_spec=pltpu.PrefetchScalarGridSpec(num_s...]
  transfers between devices with their start and end apart: 12 -> 12, of which waited for: 7 -> 7; matrix products, arithmetic and copies ran while one was open for 1% -> 1% of each run, Pallas kernels for 22% -> 19%
where the time goes in v1:
time: 77.2 us; the launch traced here: 76.8 us
  waiting for transfers between devices  27.5 us (36%)
  starting transfers between devices  25.4 us (33%)
  Pallas kernels  21.3 us (28%)
  other arithmetic  1.02 us (1%)
  between operations  0.79 us (1%)
  local copies, waits for them, and re-layouts  0.78 us (1%)
    ppermute x3, waiting for transfers between devices, local(): everyone.append(lax.ppermute(held, 'ep', far_by(bit)))  18.3 us
    ppermute x4, starting transfers between devices, local(): arrived.append(lax.ppermute(rows, ('ep', 'core'), pairs))  9.51 us
    pallas_call x1, Pallas kernels, local_recurrence(): pl.pallas_call(functools.partial(gates_kernel, first, count, len(weights)...  9.17 us
    all_to_all x1, starting transfers between devices, local(): lax.all_to_all(keep.reshape(experts * planes, capacity, model), ('ep', 'p...  5.6 us
    pallas_call x1, Pallas kernels, add_carries(): pl.pallas_call(carry_kernel, grid_spec=pltpu.PrefetchScalarGridSpec(num_s...  5.07 us
    ppermute x3, starting transfers between devices, local(): everyone.append(lax.ppermute(held, 'ep', far_by(bit)))  4.42 us
    ppermute x1, starting transfers between devices, local(): before = lax.ppermute(x_path[length - 2:], 'ep', up)  4.3 us
    ppermute x1, waiting for transfers between devices, local(): after = lax.ppermute(x_path[:2], 'ep', down)  4.18 us
  transfers between devices with their start and end apart: 12, of which 7 were waited for; matrix products, arithmetic and copies ran while one was open for 1% of the time, Pallas kernels for 19%

profile of v1, /device:TPU:0, one launch (start us, length us, event | category | flops | bytes accessed | tf_op | source)
XLA Modules:
  0.0 76.8 jit_solution(15312524930062793706)
XLA Ops:
  0.6 0.1 pad_add_fusion.ids_ref
  0.7 2.1 %prepare.1 = (bf16[2,16,64]{2,1,0:T(8,128)(2,1)S(1)}, bf16[32,2048]{1,0:T(8,128)(2,1)S(1)}, bf16[32,2048]{1,0:T(8,128)(2,1)S(1)}, bf16[32,2048]{1,0:T(8,128)(2,1)S(1)}, bf16[32,2048]{1,0:T(8,128)(2,1)S(1)}) custom-call(s32[3]{0:T(128)S(1)} %pad_add_fusion.ids_ref, bf16[64,2048]{1,0:T(8,128)(2,1)} %in_ref.1, f32[1,2048]{1,0:T(1,128)} %bitcast.17, ...), custom_call_target="tpu_custom_call" | custom-call | tf_op jit(solution)/shard_map/prepare/pallas_call | solution.py:365
  2.8 3.0 %collective-permute-start.2 = (bf16[32,2048]{1,0:T(8,128)(2,1)S(1)}, bf16[32,2048]{1,0:T(8,128)(2,1)S(1)}, u32[]{:S(2)}, u32[]{:S(2)}) collective-permute-start(bf16[32,2048]{1,0:T(8,128)(2,1)S(1)} %get-tuple-element.26), channel_id=1, source_target_pairs={{0,4},{1,21},{4,0},{5,17},{8,12},{9,29},{12,8},{13,25},{16,20},{17... | collective-permute-start | bytes 393224 | tf_op jit(solution)/shard_map/ppermute | solution.py:499
  5.8 1.6 %collective-permute-start.3 = (bf16[32,2048]{1,0:T(8,128)(2,1)S(1)}, bf16[32,2048]{1,0:T(8,128)(2,1)S(1)}, u32[]{:S(2)}, u32[]{:S(2)}) collective-permute-start(bf16[32,2048]{1,0:T(8,128)(2,1)S(1)} %get-tuple-element.27), channel_id=1, source_target_pairs={{0,8},{1,25},{4,12},{5,29},{8,0},{9,17},{12,4},{13,21},{16,24},{17... | collective-permute-start | bytes 393224 | tf_op jit(solution)/shard_map/ppermute | solution.py:499
  7.4 0.0 collective-permute-start.4
  7.4 4.9 %collective-permute-start.5 = (bf16[32,2048]{1,0:T(8,128)(2,1)S(1)}, bf16[32,2048]{1,0:T(8,128)(2,1)S(1)}, u32[]{:S(2)}, u32[]{:S(2)}) collective-permute-start(bf16[32,2048]{1,0:T(8,128)(2,1)S(1)} %get-tuple-element.29), channel_id=1, source_target_pairs={{0,16},{1,1},{4,20},{5,5},{8,24},{9,9},{12,28},{13,13},{16,0},{17,... | collective-permute-start | bytes 393224 | tf_op jit(solution)/shard_map/ppermute | solution.py:499
  12.3 0.7 fusion.1
  13.0 1.3 %collective-permute-start.1 = (bf16[2,512]{1,0:T(2,128)(2,1)S(1)}, bf16[2,512]{1,0:T(2,128)(2,1)S(1)}, u32[]{:S(2)}, u32[]{:S(2)}) collective-permute-start(bf16[2,512]{1,0:T(2,128)(2,1)S(1)} %get-tuple-element.42), channel_id=1, source_target_pairs={{4,0},{8,4},{12,8},{16,12},{20,16},{24,20},{28,24},{5,1},{9,5},{13... | collective-permute-start | bytes 6152 | tf_op jit(solution)/shard_map/ppermute | solution.py:481
  14.3 4.2 %collective-permute-done.1.refs_2_ = bf16[2,512]{1,0:T(2,128)(2,1)S(1)} collective-permute-done((bf16[2,512]{1,0:T(2,128)(2,1)S(1)}, bf16[2,512]{1,0:T(2,128)(2,1)S(1)}, u32[]{:S(2)}, u32[]{:S(2)}) %collective-permute-start.1) | collective-permute-done | bytes 2080 | tf_op jit(solution)/shard_map/ppermute | solution.py:481
  18.5 4.3 %collective-permute-start = (bf16[2,512]{1,0:T(2,128)(2,1)S(1)}, bf16[2,512]{1,0:T(2,128)(2,1)S(1)}, u32[]{:S(2)}, u32[]{:S(2)}) collective-permute-start(bf16[2,512]{1,0:T(2,128)(2,1)S(1)} %get-tuple-element.43), channel_id=1, source_target_pairs={{0,4},{4,8},{8,12},{12,16},{16,20},{20,24},{24,28},{1,5},{5,9},{9,... | collective-permute-start | bytes 6152 | tf_op jit(solution)/shard_map/ppermute | solution.py:480
  22.8 1.3 %collective-permute-done.refs_1_ = bf16[2,512]{1,0:T(2,128)(2,1)S(1)} collective-permute-done((bf16[2,512]{1,0:T(2,128)(2,1)S(1)}, bf16[2,512]{1,0:T(2,128)(2,1)S(1)}, u32[]{:S(2)}, u32[]{:S(2)}) %collective-permute-start) | collective-permute-done | bytes 2080 | tf_op jit(solution)/shard_map/ppermute | solution.py:480
  24.1 9.2 %recurrence.1 = (bf16[1024,512]{1,0:T(8,128)(2,1)}, bf16[1024,512]{1,0:T(8,128)(2,1)}, bf16[1024,512]{1,0:T(8,128)(2,1)}, f32[4,8,512]{2,1,0:T(8,128)}, f32[4,51...) custom-call(bf16[1024,512]{1,0:T(8,128)(2,1)} %refs_0_.1, ...), custom_call_target="tpu_custom_call" | custom-call | tf_op jit(solution)/shard_map/recurrence/pallas_call | solution.py:179
  33.3 0.0 collective-permute-done.2
  33.3 0.0 collective-permute-done.3
  33.3 0.0 collective-permute-done.4
  33.3 0.0 collective-permute-done.5
  33.4 0.1 collective-permute-start.9
  33.5 1.9 %collective-permute-done.9.other_ref = bf16[128,2048]{1,0:T(8,128)(2,1)S(1)} collective-permute-done((bf16[128,2048]{1,0:T(8,128)(2,1)S(1)}, bf16[128,2048]{1,0:T(8,128)(2,1)S(1)}, u32[]{:S(2)}, u32[]{:S(2)}) %collective-permute-start.9) | collective-permute-done | bytes 524320 | tf_op jit(solution)/shard_map/ppermute | solution.py:516
  35.4 4.1 %experts.1 = (bf16[128,2048]{1,0:T(8,128)(2,1)S(1)}, bf16[128,2048]{1,0:T(8,128)(2,1)S(1)}) custom-call(s32[3]{0:T(128)S(1)} %pad_add_fusion.ids_ref, bf16[128,2048]{1,0:T(8,128)(2,1)S(1)} %constant_dynamic-update-slice_fusion.own_ref, bf16[128,2048]{1,0:T(8,128)(2,1)S(1)} %collective-permute-done.9.other_ref, ...), custom_call_target="tpu_custom_call" | custom-call | tf_op jit(solution)/shard_map/experts/pallas_call | solution.py:416
  39.5 0.2 collective-permute-start.10
  39.7 1.8 %collective-permute-done.10 = bf16[128,2048]{1,0:T(8,128)(2,1)S(1)} collective-permute-done((bf16[128,2048]{1,0:T(8,128)(2,1)S(1)}, bf16[128,2048]{1,0:T(8,128)(2,1)S(1)}, u32[]{:S(2)}, u32[]{:S(2)}) %collective-permute-start.10) | collective-permute-done | bytes 524320 | tf_op jit(solution)/shard_map/ppermute | solution.py:524
  41.5 0.9 %fusion = bf16[16,8,2048]{2,1,0:T(8,128)(2,1)} fusion(bf16[128,2048]{1,0:T(8,128)(2,1)S(1)} %collective-permute-done.10, bf16[128,2048]{1,0:T(8,128)(2,1)S(1)} %get-tuple-element.39), kind=kLoop, calls=%fused_computation.1 | loop fusion | flops 1048576 | bytes 1572864 | tf_op jit(solution)/shard_map/reshape | solution.py:527
  42.4 5.6 %all-to-all-start = ((bf16[16,8,2048]{2,1,0:T(8,128)(2,1)}), bf16[16,8,2048]{2,1,0:T(8,128)(2,1)S(1)}, u32[]{:S(2)}, u32[]{:S(2)}) async-start(bf16[16,8,2048]{2,1,0:T(8,128)(2,1)} %fusion), calls=%async_computation | async-start | bytes 1048576 | tf_op jit(solution)/shard_map/all_to_all | solution.py:526
  48.0 2.9 %collective-permute-start.6 = (f32[1,4,512]{2,1,0:T(4,128)S(1)}, f32[1,4,512]{2,1,0:T(4,128)S(1)}, u32[]{:S(2)}, u32[]{:S(2)}) collective-permute-start(f32[1,4,512]{2,1,0:T(4,128)S(1)} %bitcast.12), channel_id=1, source_target_pairs={{0,16},{4,20},{8,24},{12,28},{16,0},{20,4},{24,8},{28,12},{1,17},{... | collective-permute-start | bytes 24584 | tf_op jit(solution)/shard_map/ppermute | solution.py:521
  50.9 12.1 %collective-permute-done.6.refs_1_ = f32[1,4,512]{2,1,0:T(4,128)S(1)} collective-permute-done((f32[1,4,512]{2,1,0:T(4,128)S(1)}, f32[1,4,512]{2,1,0:T(4,128)S(1)}, u32[]{:S(2)}, u32[]{:S(2)}) %collective-permute-start.6) | collective-permute-done | bytes 8224 | tf_op jit(solution)/shard_map/ppermute | solution.py:521
  63.1 0.0 collective-permute-start.7
  63.1 3.7 %collective-permute-done.7.refs_2_ = f32[2,4,512]{2,1,0:T(4,128)S(1)} collective-permute-done((f32[2,4,512]{2,1,0:T(4,128)S(1)}, f32[2,4,512]{2,1,0:T(4,128)S(1)}, u32[]{:S(2)}, u32[]{:S(2)}) %collective-permute-start.7) | collective-permute-done | bytes 16416 | tf_op jit(solution)/shard_map/ppermute | solution.py:521
  66.8 1.5 %collective-permute-start.8 = (f32[4,4,512]{2,1,0:T(4,128)S(1)}, f32[4,4,512]{2,1,0:T(4,128)S(1)}, u32[]{:S(2)}, u32[]{:S(2)}) collective-permute-start(f32[4,4,512]{2,1,0:T(4,128)S(1)} %pad_maximum_fusion), channel_id=1, source_target_pairs={{0,4},{4,0},{8,12},{12,8},{16,20},{20,16},{24,28},{28,24},{1,5},{5... | collective-permute-start | bytes 98312 | tf_op jit(solution)/shard_map/ppermute | solution.py:521
  68.3 2.5 %collective-permute-done.8.refs_3_ = f32[4,4,512]{2,1,0:T(4,128)S(1)} collective-permute-done((f32[4,4,512]{2,1,0:T(4,128)S(1)}, f32[4,4,512]{2,1,0:T(4,128)S(1)}, u32[]{:S(2)}, u32[]{:S(2)}) %collective-permute-start.8) | collective-permute-done | bytes 32800 | tf_op jit(solution)/shard_map/ppermute | solution.py:521
  70.8 5.1 %carries.1 = bf16[1024,512]{1,0:T(8,128)(2,1)} custom-call(s32[1]{0:T(128)} %bitcast.place_ref, bf16[1024,512]{1,0:T(8,128)(2,1)} %gate_ref.1, bf16[1024,512]{1,0:T(8,128)(2,1)} %get-tuple-element.22.local_ref, bf16[1024,512]{1,0:T(8,128)(2,1)} %get-tuple-element.23.forward_ref, bf16[1024,512]{1,0:T(8,128)(2,1)} %get-tuple-element.24.backward_ref, ...), custom_call_target="tpu_custom_call" | custom-call | tf_op jit(solution)/shard_map/carries/pallas_call | solution.py:289
  75.9 0.0 all-to-all-done
  75.9 0.9 %combine.1 = bf16[16,2048]{1,0:T(8,128)(2,1)} custom-call(bf16[8,2,8,2048]{3,2,1,0:T(8,128)(2,1)S(1)} %bitcast.11, bf16[2,16,64]{2,1,0:T(8,128)(2,1)S(1)} %get-tuple-element.41.share_ref), custom_call_target="tpu_custom_call" | custom-call | tf_op jit(solution)/shard_map/combine/pallas_call | solution.py:440
  (10 shorter events, 0.1 us)
Async XLA Ops:
  2.8 30.5 %collective-permute-start.2 = (bf16[32,2048]{1,0:T(8,128)(2,1)S(1)}, bf16[32,2048]{1,0:T(8,128)(2,1)S(1)}, u32[]{:S(2)}, u32[]{:S(2)}) collective-permute-start(bf16[32,2048]{1,0:T(8,128)(2,1)S(1)} %get-tuple-element.26), channel_id=1, source_target_pairs={{0,4},{1,21},{4,0},{5,17},{8,12},{9,29},{12,8},{13,25},{16,20},{17... | collective-permute-start | bytes 393224 | tf_op jit(solution)/shard_map/ppermute | solution.py:499
  5.8 27.5 %collective-permute-start.3 = (bf16[32,2048]{1,0:T(8,128)(2,1)S(1)}, bf16[32,2048]{1,0:T(8,128)(2,1)S(1)}, u32[]{:S(2)}, u32[]{:S(2)}) collective-permute-start(bf16[32,2048]{1,0:T(8,128)(2,1)S(1)} %get-tuple-element.27), channel_id=1, source_target_pairs={{0,8},{1,25},{4,12},{5,29},{8,0},{9,17},{12,4},{13,21},{16,24},{17... | collective-permute-start | bytes 393224 | tf_op jit(solution)/shard_map/ppermute | solution.py:499
  7.4 25.9 %collective-permute-start.4 = (bf16[32,2048]{1,0:T(8,128)(2,1)S(1)}, bf16[32,2048]{1,0:T(8,128)(2,1)S(1)}, u32[]{:S(2)}, u32[]{:S(2)}) collective-permute-start(bf16[32,2048]{1,0:T(8,128)(2,1)S(1)} %get-tuple-element.28), channel_id=1, source_target_pairs={{0,12},{1,29},{4,8},{5,25},{8,4},{9,21},{12,0},{13,17},{16,28},{17... | collective-permute-start | bytes 393224 | tf_op jit(solution)/shard_map/ppermute | solution.py:499
  7.4 25.9 %collective-permute-start.5 = (bf16[32,2048]{1,0:T(8,128)(2,1)S(1)}, bf16[32,2048]{1,0:T(8,128)(2,1)S(1)}, u32[]{:S(2)}, u32[]{:S(2)}) collective-permute-start(bf16[32,2048]{1,0:T(8,128)(2,1)S(1)} %get-tuple-element.29), channel_id=1, source_target_pairs={{0,16},{1,1},{4,20},{5,5},{8,24},{9,9},{12,28},{13,13},{16,0},{17,... | collective-permute-start | bytes 393224 | tf_op jit(solution)/shard_map/ppermute | solution.py:499
  13.0 5.5 %collective-permute-start.1 = (bf16[2,512]{1,0:T(2,128)(2,1)S(1)}, bf16[2,512]{1,0:T(2,128)(2,1)S(1)}, u32[]{:S(2)}, u32[]{:S(2)}) collective-permute-start(bf16[2,512]{1,0:T(2,128)(2,1)S(1)} %get-tuple-element.42), channel_id=1, source_target_pairs={{4,0},{8,4},{12,8},{16,12},{20,16},{24,20},{28,24},{5,1},{9,5},{13... | collective-permute-start | bytes 6152 | tf_op jit(solution)/shard_map/ppermute | solution.py:481
  18.5 5.6 %collective-permute-start = (bf16[2,512]{1,0:T(2,128)(2,1)S(1)}, bf16[2,512]{1,0:T(2,128)(2,1)S(1)}, u32[]{:S(2)}, u32[]{:S(2)}) collective-permute-start(bf16[2,512]{1,0:T(2,128)(2,1)S(1)} %get-tuple-element.43), channel_id=1, source_target_pairs={{0,4},{4,8},{8,12},{12,16},{16,20},{20,24},{24,28},{1,5},{5,9},{9,... | collective-permute-start | bytes 6152 | tf_op jit(solution)/shard_map/ppermute | solution.py:480
  33.4 2.0 %collective-permute-start.9 = (bf16[128,2048]{1,0:T(8,128)(2,1)S(1)}, bf16[128,2048]{1,0:T(8,128)(2,1)S(1)}, u32[]{:S(2)}, u32[]{:S(2)}) collective-permute-start(bf16[128,2048]{1,0:T(8,128)(2,1)S(1)} %constant_dynamic-update-slice_fusion.own_ref), channel_id=1, source_target_pairs={{0,1},{1,0},{2,3},{3,2},{4,5},{5,4},{6,7},{7,6},{8,9},{9,8},{10,11... | collective-permute-start | bytes 1572872 | tf_op jit(solution)/shard_map/ppermute | solution.py:516
  35.4 12.6 %copy-start = (f32[4,512]{1,0:T(4,128)S(1)}, f32[4,512]{1,0:T(4,128)}, u32[]{:S(2)}) copy-start(f32[4,512]{1,0:T(4,128)} %get-tuple-element.31) | copy-start | bytes 24580
  35.4 35.4 %copy-start.1 = (f32[4,8,512]{2,1,0:T(8,128)S(1)}, f32[4,8,512]{2,1,0:T(8,128)}, u32[]{:S(2)}) copy-start(f32[4,8,512]{2,1,0:T(8,128)} %get-tuple-element.25.chunk_ref) | copy-start | bytes 196612
  39.5 2.0 %collective-permute-start.10 = (bf16[128,2048]{1,0:T(8,128)(2,1)S(1)}, bf16[128,2048]{1,0:T(8,128)(2,1)S(1)}, u32[]{:S(2)}, u32[]{:S(2)}) collective-permute-start(bf16[128,2048]{1,0:T(8,128)(2,1)S(1)} %get-tuple-element.40), channel_id=1, source_target_pairs={{0,1},{1,0},{2,3},{3,2},{4,5},{5,4},{6,7},{7,6},{8,9},{9,8},{10,11... | collective-permute-start | bytes 1572872 | tf_op jit(solution)/shard_map/ppermute | solution.py:524
  42.4 33.5 %all-to-all-start = ((bf16[16,8,2048]{2,1,0:T(8,128)(2,1)}), bf16[16,8,2048]{2,1,0:T(8,128)(2,1)S(1)}, u32[]{:S(2)}, u32[]{:S(2)}) async-start(bf16[16,8,2048]{2,1,0:T(8,128)(2,1)} %fusion), calls=%async_computation | async-start | bytes 1048576 | tf_op jit(solution)/shard_map/all_to_all | solution.py:526
  48.0 15.0 %collective-permute-start.6 = (f32[1,4,512]{2,1,0:T(4,128)S(1)}, f32[1,4,512]{2,1,0:T(4,128)S(1)}, u32[]{:S(2)}, u32[]{:S(2)}) collective-permute-start(f32[1,4,512]{2,1,0:T(4,128)S(1)} %bitcast.12), channel_id=1, source_target_pairs={{0,16},{4,20},{8,24},{12,28},{16,0},{20,4},{24,8},{28,12},{1,17},{... | collective-permute-start | bytes 24584 | tf_op jit(solution)/shard_map/ppermute | solution.py:521
  63.1 3.7 %collective-permute-start.7 = (f32[2,4,512]{2,1,0:T(4,128)S(1)}, f32[2,4,512]{2,1,0:T(4,128)S(1)}, u32[]{:S(2)}, u32[]{:S(2)}) collective-permute-start(f32[2,4,512]{2,1,0:T(4,128)S(1)} %pad_maximum_fusion.1), channel_id=1, source_target_pairs={{0,8},{4,12},{8,0},{12,4},{16,24},{20,28},{24,16},{28,20},{1,9},{5... | collective-permute-start | bytes 49160 | tf_op jit(solution)/shard_map/ppermute | solution.py:521
  66.8 4.0 %collective-permute-start.8 = (f32[4,4,512]{2,1,0:T(4,128)S(1)}, f32[4,4,512]{2,1,0:T(4,128)S(1)}, u32[]{:S(2)}, u32[]{:S(2)}) collective-permute-start(f32[4,4,512]{2,1,0:T(4,128)S(1)} %pad_maximum_fusion), channel_id=1, source_target_pairs={{0,4},{4,0},{8,12},{12,8},{16,20},{20,16},{24,28},{28,24},{1,5},{5... | collective-permute-start | bytes 98312 | tf_op jit(solution)/shard_map/ppermute | solution.py:521

commit v2 on v1

--- a/solution.py
+++ b/solution.py
@@ -14,6 +14,7 @@
 LANES = 128
 CHUNKS = 8
 STEPS = 64
+TILE = 16
 LOG2E = math.log2(math.e)
 LN2 = math.log(2.0)
 SERIES = (-2.0 * LN2, -((2.0 * LN2) ** 2) / 2.0, -((2.0 * LN2) ** 3) / 6.0)
@@ -23,9 +24,33 @@
     return pltpu.with_memory_space_constraint(x, pltpu.HBM)
 
 
+def gate_weights(decay_w_ref, input_w_ref):
+    return jnp.concatenate(
+        [decay_w_ref[0, 0], input_w_ref[0, 0], decay_w_ref[1, 0], input_w_ref[1, 0]], axis=1
+    )
+
+
+def decays_and_drives(conv_sum, weights, slopes, moved):
+    f32 = jnp.float32
+    conv = conv_sum.astype(jnp.bfloat16)
+    wide = jnp.dot(conv * jnp.bfloat16(0.5), weights, preferred_element_type=f32)
+    half = conv.astype(f32) * 0.5
+    found = []
+    for d in range(2):
+        decay_t = jnp.tanh(wide[:, 2 * d * LANES : (2 * d + 1) * LANES])
+        input_t = jnp.tanh(wide[:, (2 * d + 1) * LANES : (2 * d + 2) * LANES])
+        power = slopes[d] * decay_t + (moved + slopes[d])
+        decay = jnp.exp2(power)
+        small = power * (SERIES[0] + power * (SERIES[1] + power * SERIES[2]))
+        lost = jnp.where(power > -0.03125, small, 1.0 - decay * decay)
+        root = lost * lax.rsqrt(jnp.maximum(lost, 1e-37))
+        found.append((decay, root * (input_t + 1.0) * half))
+    return found
+
+
 def gates_kernel(first, count, fetched, filled, *refs):
-    x_ref, before_ref, after_ref, taps_ref, decay_w_ref, input_w_ref, rate_ref, shift_ref = refs[:8]
-    at = 8
+    x_ref, taps_ref, decay_w_ref, input_w_ref, rate_ref, shift_ref = refs[:6]
+    at = 6
     sources = refs[at : at + fetched]
     at += fetched + filled
     local_ref, forward_ref, backward_ref, chunk_ref, total_ref = refs[at : at + 5]
@@ -62,20 +87,22 @@
             rows_ref[(s + 1) * pitch : (s + 1) * pitch + 2, :] = block[per - 2 : per]
         if s > 0:
             rows_ref[(s - 1) * pitch + per + 2 : (s - 1) * pitch + per + 3, :] = block[0:1]
-    rows_ref[0:2, :] = before_ref[...].astype(f32)
+    rows_ref[0:2, :] = jnp.zeros((2, LANES), f32)
     last = (CHUNKS - 1) * pitch + per + 2
-    rows_ref[last : last + 1, :] = after_ref[0:1, :].astype(f32)
+    rows_ref[last : last + 1, :] = jnp.zeros((1, LANES), f32)
 
     taps = [jnp.broadcast_to(taps_ref[k : k + 1, :], (CHUNKS, LANES)) for k in range(4)]
-    weights = jnp.concatenate(
-        [decay_w_ref[0, 0], input_w_ref[0, 0], decay_w_ref[1, 0], input_w_ref[1, 0]], axis=1
-    )
+    weights = gate_weights(decay_w_ref, input_w_ref)
     head = pl.program_id(0) + first
     here = lax.broadcasted_iota(jnp.int32, shift_ref.shape, 0) == head
     shift = jnp.sum(jnp.where(here, shift_ref[...], 0.0), axis=0, keepdims=True) * LOG2E
     shift = jnp.concatenate([shift[:, s * per : (s + 1) * per] for s in range(CHUNKS)], axis=0)
     slopes = [rate_ref[d : d + 1, :] * (-4.0 * LOG2E) for d in range(2)]
     size = STEPS * CHUNKS
+
+    blocks = per // STEPS
+    chunk = lax.broadcasted_iota(jnp.int32, (CHUNKS, LANES), 0)
+    top, bottom = chunk == 0, chunk == CHUNKS - 1
 
     def gates(b, carry):
         state, prod = carry
@@ -87,32 +114,29 @@
             for k in range(1, 4):
                 total = total + taken[i + k] * taps[k]
             sums.append(total)
-        conv = jnp.concatenate(sums, axis=0).astype(jnp.bfloat16)
-        wide = jnp.dot(conv * jnp.bfloat16(0.5), weights, preferred_element_type=f32)
-        half = conv.astype(f32) * 0.5
         turned = pltpu.roll(shift, lax.rem(per - base, per), axis=1)
         moved = jnp.concatenate(
             [jnp.broadcast_to(turned[:, i : i + 1], (CHUNKS, LANES)) for i in range(STEPS)], axis=0
         )
         start = pl.multiple_of(b * size, size)
-        for d in range(2):
-            decay_t = jnp.tanh(wide[:, 2 * d * LANES : (2 * d + 1) * LANES])
-            input_t = jnp.tanh(wide[:, (2 * d + 1) * LANES : (2 * d + 2) * LANES])
-            power = slopes[d] * decay_t + (moved + slopes[d])
-            decay = jnp.exp2(power)
-            small = power * (SERIES[0] + power * (SERIES[1] + power * SERIES[2]))
-            lost = jnp.where(power > -0.03125, small, 1.0 - decay * decay)
-            root = lost * lax.rsqrt(jnp.maximum(lost, 1e-37))
-            drive = root * (input_t + 1.0) * half
+        found = decays_and_drives(jnp.concatenate(sums, axis=0), weights, slopes, moved)
+        for d, (decay, drive) in enumerate(found):
             if d == 0:
                 for i in range(STEPS):
                     step = decay[i * CHUNKS : (i + 1) * CHUNKS]
+                    held = state, prod
                     state = step * state + drive[i * CHUNKS : (i + 1) * CHUNKS]
+                    prod = step * prod
+                    if i == 1:
+                        edge = top & (b == 0)
+                        state, prod = jnp.where(edge, 0.0, state), jnp.where(edge, 1.0, prod)
+                    if i == STEPS - 1:
+                        edge = bottom & (b == blocks - 1)
+                        state, prod = jnp.where(edge, held[0], state), jnp.where(edge, held[1], prod)
                     state_ref[pl.ds(start + i * CHUNKS, CHUNKS), :] = state
-                    held, prod = prod, step * prod
                     if i % 2:
                         two = pl.ds(start + (i - 1) * CHUNKS, 2 * CHUNKS)
-                        forward_ref[two, :] = jnp.concatenate([held, prod]).astype(forward_ref.dtype)
+                        forward_ref[two, :] = jnp.concatenate([held[1], prod]).astype(forward_ref.dtype)
             else:
                 decay_ref[pl.ds(start, size), :] = decay
                 drive_ref[pl.ds(start, size), :] = drive
@@ -120,7 +144,6 @@
 
     zero = jnp.zeros((CHUNKS, LANES), f32)
     one = jnp.ones((CHUNKS, LANES), f32)
-    blocks = per // STEPS
     forward_end, forward_prod = lax.fori_loop(0, blocks, gates, (zero, one))
 
     def back(b, carry):
@@ -130,8 +153,15 @@
         for i in reversed(range(STEPS)):
             at = pl.ds(start + i * CHUNKS, CHUNKS)
             step = decay_ref[at, :]
+            held = state, prod
             state = step * state + drive_ref[at, :]
             prod = step * prod
+            if i == STEPS - 1:
+                edge = bottom & (b == 0)
+                state, prod = jnp.where(edge, 0.0, state), jnp.where(edge, 1.0, prod)
+            if i < 2:
+                edge = top & (b == blocks - 1)
+                state, prod = jnp.where(edge, held[0], state), jnp.where(edge, held[1], prod)
             total = state + state_ref[at, :]
             if i % 2:
                 last_total, last_prod = total, prod
@@ -151,14 +181,27 @@
     for s in range(CHUNKS):
         state = forward_prod[s : s + 1] * state + forward_end[s : s + 1]
         prod = prod * forward_prod[s : s + 1]
-    total_ref[0:1, :] = prod
-    total_ref[1:2, :] = state
+    total_ref[0, 0:1, :] = prod
+    total_ref[0, 1:2, :] = state
     state, prod = zero[0:1], one[0:1]
     for s in reversed(range(CHUNKS)):
         state = backward_prod[s : s + 1] * state + backward_end[s : s + 1]
         prod = prod * backward_prod[s : s + 1]
-    total_ref[2:3, :] = prod
-    total_ref[3:4, :] = state
+    total_ref[0, 2:3, :] = prod
+    total_ref[0, 3:4, :] = state
+    head_rows = x_ref[0:TILE, :].astype(f32)
+    tail_rows = x_ref[length - TILE : length, :].astype(f32)
+    for r in range(3):
+        total_ref[(4 + r) // 4, (4 + r) % 4 : (4 + r) % 4 + 1, :] = head_rows[r : r + 1]
+        end = TILE - 3 + r
+        total_ref[(7 + r) // 4, (7 + r) % 4 : (7 + r) % 4 + 1, :] = tail_rows[end : end + 1]
+    lane = lax.broadcasted_iota(jnp.int32, (1, LANES), 1)
+    total_ref[2, 2:3, :] = jnp.where(
+        lane == 0,
+        shift[0:1, 0:1],
+        jnp.where(lane == 1, shift[0:1, 1:2], shift[CHUNKS - 1 : CHUNKS, per - 1 : per]),
+    )
+    total_ref[2, 3:4, :] = zero[0:1]
 
     @pl.when(pl.program_id(0) == pl.num_programs(0) - 1)
     def _():
@@ -168,7 +211,7 @@
 
 
 def local_recurrence(first, count, arrays, weights, partial):
-    x, before, after, taps, decay_w, input_w, rate, shift = arrays
+    x, taps, decay_w, input_w, rate, shift = arrays
     length, channels = x.shape
     heads = decay_w.shape[1]
     per = length // CHUNKS
@@ -181,8 +224,6 @@
         grid=(count,),
         in_specs=[
             pl.BlockSpec((length, LANES), col),
-            pl.BlockSpec((2, LANES), col),
-            pl.BlockSpec((2, LANES), col),
             pl.BlockSpec((4, LANES), col),
             pl.BlockSpec((2, 1, LANES, LANES), lambda h: (0, h + first, 0, 0)),
             pl.BlockSpec((2, 1, LANES, LANES), lambda h: (0, h + first, 0, 0)),
@@ -195,7 +236,7 @@
             pl.BlockSpec((length, LANES), col),
             pl.BlockSpec((length, LANES), col),
             pl.BlockSpec((4, CHUNKS, LANES), lambda h: (0, 0, h + first)),
-            pl.BlockSpec((4, LANES), col),
+            pl.BlockSpec((3, 4, LANES), lambda h: (0, 0, h + first)),
         ]
         + [pl.BlockSpec(memory_space=pltpu.VMEM)] * len(weights),
         out_shape=[
@@ -203,7 +244,7 @@
             pltpu.HBM((length, channels), bf16),
             pltpu.HBM((length, channels), bf16),
             pltpu.HBM((4, CHUNKS, channels), f32),
-            pltpu.HBM((4, channels), f32),
+            pltpu.HBM((3, 4, channels), f32),
         ]
         + [pltpu.VMEM(w.shape[1:], w.dtype) for w in weights],
         scratch_shapes=[
@@ -213,45 +254,108 @@
             pltpu.VMEM((length, LANES), f32),
             pltpu.SemaphoreType.DMA((3, count)),
         ],
-        input_output_aliases={8 + len(weights) + i: i for i in range(len(partial))},
+        input_output_aliases={6 + len(weights) + i: i for i in range(len(partial))},
         compiler_params=pltpu.CompilerParams(vmem_limit_bytes=20 << 20),
         name="recurrence",
     )(
-        far(x), before, after, far(taps), far(decay_w), far(input_w), far(rate), far(shift.T),
+        far(x), far(taps), far(decay_w), far(input_w), far(rate), far(shift.T),
         *map(far, weights), *map(far, partial)
     )
     return list(outs[:5]), list(outs[5:])
 
 
-def carry_kernel(place_ref, gate_ref, local_ref, forward_ref, backward_ref, chunk_ref, *refs):
+def carry_kernel(
+    place_ref,
+    gate_ref,
+    local_ref,
+    forward_ref,
+    backward_ref,
+    chunk_ref,
+    taps_ref,
+    decay_w_ref,
+    input_w_ref,
+    rate_ref,
+    *refs,
+):
     *pieces, out_ref, all_ref, ends_ref, rows_ref = refs
     length = local_ref.shape[0]
     per = length // CHUNKS
     pitch = per + 4
     f32 = jnp.float32
     place = place_ref[0]
-    count = all_ref.shape[0]
+    count = all_ref.shape[1]
     away, bit = [0], count // 2
-    all_ref[0] = pieces[0][0]
-    for piece in pieces[1:]:
-        for i, d in enumerate(away):
-            all_ref[d ^ bit] = piece[i]
-        away += [d ^ bit for d in away]
-        bit //= 2
-    carry = jnp.zeros((1, LANES), f32)
+    for i, piece in enumerate(pieces):
+        start = 0 if i == 0 else len(away)
+        if i:
+            away += [d ^ bit for d in away]
+            bit //= 2
+        for j in range(piece.shape[0]):
+            at = pl.ds(away[start + j] ^ place, 1)
+            for r in range(11):
+                all_ref[r, at, :] = piece[j, r // 4, r % 4 : r % 4 + 1, :]
+    parts = [all_ref[r] for r in range(11)]
+    prod_f, end_f, prod_b, end_b = parts[:4]
+    head, tail, shift = parts[4:7], parts[7:10], parts[10]
+    none = jnp.zeros((1, LANES), f32)
+    earlier = lambda v: jnp.concatenate([none, v[:-1]], axis=0)
+    later = lambda v: jnp.concatenate([v[1:], none], axis=0)
+    spans = (
+        (earlier(tail[1]), earlier(tail[2]), head[0], head[1]),
+        (earlier(tail[2]), head[0], head[1], head[2]),
+        (tail[0], tail[1], tail[2], later(head[0])),
+    )
+    sums = []
+    for span in spans:
+        total = span[0] * taps_ref[0:1, :]
+        for k in range(1, 4):
+            total = total + span[k] * taps_ref[k : k + 1, :]
+        sums.append(total)
+    moved = [jnp.broadcast_to(shift[:, r : r + 1], (count, LANES)) for r in range(3)]
+    spare = -3 * count % TILE
+    if spare:
+        sums.append(jnp.zeros((spare, LANES), f32))
+        moved.append(jnp.zeros((spare, LANES), f32))
+    slopes = [rate_ref[d : d + 1, :] * (-4.0 * LOG2E) for d in range(2)]
+    edges = []
+    for found in decays_and_drives(
+        jnp.concatenate(sums, axis=0),
+        gate_weights(decay_w_ref, input_w_ref),
+        slopes,
+        jnp.concatenate(moved, axis=0),
+    ):
+        edges.append([[v[r * count : (r + 1) * count] for v in found] for r in range(3)])
+    (d0, u0), (d1, u1), (dz, uz) = edges[0]
+    (e0, w0), (e1, w1), (ez, wz) = edges[1]
+    own_row = lax.broadcasted_iota(jnp.int32, (count, LANES), 0) == place
+    own = lambda v: jnp.sum(jnp.where(own_row, v, 0.0), axis=0, keepdims=True)
+    whole_prod = dz * prod_f * d1 * d0
+    whole_end = dz * (prod_f * (d1 * u0 + u1) + end_f) + uz
+    carry = none
     for e in range(count):
-        after = all_ref[e ^ place, 0:1] * carry + all_ref[e ^ place, 1:2]
+        after = whole_prod[e : e + 1] * carry + whole_end[e : e + 1]
         carry = jnp.where(e < place, after, carry)
+    row_0 = own(d0) * carry + own(u0)
+    row_1 = own(d1) * row_0 + own(u1)
+    carry = row_1
     for s in range(CHUNKS):
         ends_ref[0, s : s + 1, :] = carry
         carry = chunk_ref[0, s : s + 1] * carry + chunk_ref[1, s : s + 1]
-    carry = jnp.zeros((1, LANES), f32)
+    row_z = own(dz) * carry + own(uz)
+    whole_prod = e0 * e1 * prod_b * ez
+    whole_end = e0 * (e1 * (prod_b * wz + end_b) + w1) + w0
+    carry = none
     for e in reversed(range(count)):
-        after = all_ref[e ^ place, 2:3] * carry + all_ref[e ^ place, 3:4]
+        after = whole_prod[e : e + 1] * carry + whole_end[e : e + 1]
         carry = jnp.where(e > place, after, carry)
+    carry = own(ez) * carry + own(wz)
+    row_z = row_z + carry
     for s in reversed(range(CHUNKS)):
         ends_ref[1, s : s + 1, :] = carry
         carry = chunk_ref[2, s : s + 1] * carry + chunk_ref[3, s : s + 1]
+    carry = own(e1) * carry + own(w1)
+    row_1 = row_1 + carry
+    row_0 = row_0 + own(e0) * carry + own(w0)
     ahead, behind = ends_ref[0], ends_ref[1]
     size = STEPS * CHUNKS
 
@@ -267,6 +371,10 @@
         return none
 
     lax.fori_loop(0, per // STEPS, add, 0)
+    rows_ref[0:1, :] = row_0
+    rows_ref[1:2, :] = row_1
+    last = (CHUNKS - 1) * pitch + per - 1
+    rows_ref[last : last + 1, :] = row_z
     span = 64
 
     def finish(b, none):
@@ -282,7 +390,8 @@
     lax.fori_loop(0, length // span, finish, 0)
 
 
-def add_carries(place, gate, local, forward, backward, chunks, everyone):
+def add_carries(place, gate, arrays, local, forward, backward, chunks, everyone):
+    taps, decay_w, input_w, rate = arrays
     length, channels = local.shape
     count = sum(piece.shape[0] for piece in everyone)
     col = lambda h, p: (0, h)
@@ -292,11 +401,17 @@
             num_scalar_prefetch=1,
             grid=(channels // LANES,),
             in_specs=[pl.BlockSpec((length, LANES), col)] * 4
-            + [pl.BlockSpec((4, CHUNKS, LANES), lambda h, p: (0, 0, h))]
-            + [pl.BlockSpec((len(piece), 4, LANES), lambda h, p: (0, 0, h)) for piece in everyone],
+            + [
+                pl.BlockSpec((4, CHUNKS, LANES), lambda h, p: (0, 0, h)),
+                pl.BlockSpec((4, LANES), col),
+                pl.BlockSpec((2, 1, LANES, LANES), lambda h, p: (0, h, 0, 0)),
+                pl.BlockSpec((2, 1, LANES, LANES), lambda h, p: (0, h, 0, 0)),
+                pl.BlockSpec((2, LANES), col),
+            ]
+            + [pl.BlockSpec((len(piece), 3, 4, LANES), lambda h, p: (0, 0, 0, h)) for piece in everyone],
             out_specs=pl.BlockSpec((length, LANES), col),
             scratch_shapes=[
-                pltpu.VMEM((count, 4, LANES), jnp.float32),
+                pltpu.VMEM((12, count, LANES), jnp.float32),
                 pltpu.VMEM((2, CHUNKS, LANES), jnp.float32),
                 pltpu.VMEM((length + 4 * CHUNKS, LANES), jnp.float32),
             ],
@@ -304,7 +419,10 @@
         out_shape=jax.ShapeDtypeStruct((length, channels), jnp.bfloat16),
         compiler_params=pltpu.CompilerParams(vmem_limit_bytes=20 << 20),
         name="carries",
-    )(place, far(gate), far(local), far(forward), far(backward), chunks, *everyone)
+    )(
+        place, far(gate), far(local), far(forward), far(backward), chunks,
+        far(taps), far(decay_w), far(input_w), far(rate), *everyone
+    )
 
 
 def prepare_kernel(
@@ -467,18 +585,13 @@
     place = lax.axis_index("ep")
     core = lax.axis_index("core")
     block = lax.axis_index("plane") * cores + core
-    length = x_path.shape[0]
     group_rows, model = expert_in.shape
     block_rows = group_rows // (planes * cores)
     capacity = max(2, 2 * block_rows * TOP_K // experts)
 
-    up = [(i, i + 1) for i in range(experts - 1)]
-    down = [(j, i) for i, j in up]
     swap = [(i, cores - 1 - i) for i in range(cores)]
     far_by = lambda d: [(i, i ^ d) for i in range(experts)]
     ids = jnp.stack([core, block, place]).astype(jnp.int32)
-    before = lax.ppermute(x_path[length - 2 :], "ep", up)
-    after = lax.ppermute(x_path[:2], "ep", down)
     share, *outgoing = prepare(
         ids,
         expert_in,
@@ -500,8 +613,6 @@
 
     arrays = (
         x_path,
-        before,
-        after,
         conv_taps,
         decay_gate_w,
         input_gate_w,
@@ -527,7 +638,7 @@
         keep.reshape(experts * planes, capacity, model), ("ep", "plane"), 0, 0, tiled=True
     ).reshape(experts, planes, capacity, model)
     recurrent_out = add_carries(
-        place.reshape(1).astype(jnp.int32), gate_path, mixed, forward, backward, chunks, everyone
+        place.reshape(1).astype(jnp.int32), gate_path, arrays[1:5], mixed, forward, backward, chunks, everyone
     )
     expert_out = combine(back, share)
     return (recurrent_out, expert_out)

time: 77.2 us -> 67.1 us (0.87)
  starting transfers between devices: 25.4 us -> 19.1 us
  waiting for transfers between devices: 27.5 us -> 23.8 us
    ppermute x2 -> x0, starting transfers between devices: 5.58 us -> none  [the longest x1 4.3 us: local(): before = lax.ppermute(x_path[length - 2:], 'ep', up)]
    ppermute x2 -> x0, waiting for transfers between devices: 5.47 us -> none  [the longest x1 4.18 us: local(): after = lax.ppermute(x_path[:2], 'ep', down)]
    ppermute x3, waiting for transfers between devices: 18.3 us -> 20.1 us  [local(): everyone.append(lax.ppermute(held, 'ep', far_by(bit)))]
  transfers between devices with their start and end apart: 12 -> 10, of which waited for: 7 -> 5; matrix products, arithmetic and copies ran while one was open for 1% -> 0% of each run, Pallas kernels for 19% -> 22%
where the time goes in v2:
time: 67.1 us; the launch traced here: 66.7 us
  waiting for transfers between devices  23.8 us (35%)
  Pallas kernels  22 us (33%)
  starting transfers between devices  19.1 us (28%)
  other arithmetic  1.04 us (2%)
  between operations  0.78 us (1%)
    ppermute x3, waiting for transfers between devices, local(): everyone.append(lax.ppermute(held, 'ep', far_by(bit)))  20.1 us
    ppermute x4, starting transfers between devices, local(): arrived.append(lax.ppermute(rows, ('ep', 'core'), pairs))  9.51 us
    pallas_call x1, Pallas kernels, local_recurrence(): pl.pallas_call(functools.partial(gates_kernel, first, count, len(weights)...  9.21 us
    pallas_call x1, Pallas kernels, add_carries(): pl.pallas_call(carry_kernel, grid_spec=pltpu.PrefetchScalarGridSpec(num_s...  5.77 us
    all_to_all x1, starting transfers between devices, local(): lax.all_to_all(keep.reshape(experts * planes, capacity, model), ('ep', 'p...  4.84 us
    ppermute x3, starting transfers between devices, local(): everyone.append(lax.ppermute(held, 'ep', far_by(bit)))  4.49 us
    pallas_call x1, Pallas kernels, expert(): pl.pallas_call(functools.partial(expert_kernel, groups, cores), in_specs=...  4.03 us
    pallas_call x1, Pallas kernels, prepare(): pl.pallas_call(functools.partial(prepare_kernel, block_rows=block_rows, e...  2.06 us
  transfers between devices with their start and end apart: 10, of which 5 were waited for; matrix products, arithmetic and copies ran while one was open for 0% of the time, Pallas kernels for 22%

profile of v2, /device:TPU:0, one launch (start us, length us, event | category | flops | bytes accessed | tf_op | source)
XLA Modules:
  0.0 66.7 jit_solution(14196098243832040655)
XLA Ops:
  0.6 0.1 pad_add_fusion.ids_ref
  0.7 2.1 %prepare.1 = (bf16[2,16,64]{2,1,0:T(8,128)(2,1)S(1)}, bf16[32,2048]{1,0:T(8,128)(2,1)S(1)}, bf16[32,2048]{1,0:T(8,128)(2,1)S(1)}, bf16[32,2048]{1,0:T(8,128)(2,1)S(1)}, bf16[32,2048]{1,0:T(8,128)(2,1)S(1)}) custom-call(s32[3]{0:T(128)S(1)} %pad_add_fusion.ids_ref, bf16[64,2048]{1,0:T(8,128)(2,1)} %in_ref.1, f32[1,2048]{1,0:T(1,128)} %bitcast.17, ...), custom_call_target="tpu_custom_call" | custom-call | tf_op jit(solution)/shard_map/prepare/pallas_call | solution.py:483
  2.8 3.0 %collective-permute-start = (bf16[32,2048]{1,0:T(8,128)(2,1)S(1)}, bf16[32,2048]{1,0:T(8,128)(2,1)S(1)}, u32[]{:S(2)}, u32[]{:S(2)}) collective-permute-start(bf16[32,2048]{1,0:T(8,128)(2,1)S(1)} %get-tuple-element.26), channel_id=1, source_target_pairs={{0,4},{1,21},{4,0},{5,17},{8,12},{9,29},{12,8},{13,25},{16,20},{17... | collective-permute-start | bytes 393224 | tf_op jit(solution)/shard_map/ppermute | solution.py:612
  5.8 1.6 %collective-permute-start.1 = (bf16[32,2048]{1,0:T(8,128)(2,1)S(1)}, bf16[32,2048]{1,0:T(8,128)(2,1)S(1)}, u32[]{:S(2)}, u32[]{:S(2)}) collective-permute-start(bf16[32,2048]{1,0:T(8,128)(2,1)S(1)} %get-tuple-element.27), channel_id=1, source_target_pairs={{0,8},{1,25},{4,12},{5,29},{8,0},{9,17},{12,4},{13,21},{16,24},{17... | collective-permute-start | bytes 393224 | tf_op jit(solution)/shard_map/ppermute | solution.py:612
  7.4 0.0 collective-permute-start.2
  7.4 4.9 %collective-permute-start.3 = (bf16[32,2048]{1,0:T(8,128)(2,1)S(1)}, bf16[32,2048]{1,0:T(8,128)(2,1)S(1)}, u32[]{:S(2)}, u32[]{:S(2)}) collective-permute-start(bf16[32,2048]{1,0:T(8,128)(2,1)S(1)} %get-tuple-element.29), channel_id=1, source_target_pairs={{0,16},{1,1},{4,20},{5,5},{8,24},{9,9},{12,28},{13,13},{16,0},{17,... | collective-permute-start | bytes 393224 | tf_op jit(solution)/shard_map/ppermute | solution.py:612
  12.3 9.2 %recurrence.1 = (bf16[1024,512]{1,0:T(8,128)(2,1)}, bf16[1024,512]{1,0:T(8,128)(2,1)}, bf16[1024,512]{1,0:T(8,128)(2,1)}, f32[4,8,512]{2,1,0:T(8,128)}, f32[3,4,...) custom-call(bf16[1024,512]{1,0:T(8,128)(2,1)} %refs_0_.1, ...), custom_call_target="tpu_custom_call" | custom-call | tf_op jit(solution)/shard_map/recurrence/pallas_call | solution.py:222
  21.5 0.0 collective-permute-done
  21.5 0.0 collective-permute-done.1
  21.5 0.0 collective-permute-done.2
  21.6 0.0 collective-permute-done.3
  21.6 0.1 collective-permute-start.7
  21.7 1.9 %collective-permute-done.7.other_ref = bf16[128,2048]{1,0:T(8,128)(2,1)S(1)} collective-permute-done((bf16[128,2048]{1,0:T(8,128)(2,1)S(1)}, bf16[128,2048]{1,0:T(8,128)(2,1)S(1)}, u32[]{:S(2)}, u32[]{:S(2)}) %collective-permute-start.7) | collective-permute-done | bytes 524320 | tf_op jit(solution)/shard_map/ppermute | solution.py:627
  23.6 0.0 copy-start
  23.6 0.0 copy-start.1
  23.6 4.0 %experts.1 = (bf16[128,2048]{1,0:T(8,128)(2,1)S(1)}, bf16[128,2048]{1,0:T(8,128)(2,1)S(1)}) custom-call(s32[3]{0:T(128)S(1)} %pad_add_fusion.ids_ref, bf16[128,2048]{1,0:T(8,128)(2,1)S(1)} %constant_dynamic-update-slice_fusion.own_ref, bf16[128,2048]{1,0:T(8,128)(2,1)S(1)} %collective-permute-done.7.other_ref, ...), custom_call_target="tpu_custom_call" | custom-call | tf_op jit(solution)/shard_map/experts/pallas_call | solution.py:534
  27.7 0.2 collective-permute-start.8
  27.9 1.8 %collective-permute-done.8 = bf16[128,2048]{1,0:T(8,128)(2,1)S(1)} collective-permute-done((bf16[128,2048]{1,0:T(8,128)(2,1)S(1)}, bf16[128,2048]{1,0:T(8,128)(2,1)S(1)}, u32[]{:S(2)}, u32[]{:S(2)}) %collective-permute-start.8) | collective-permute-done | bytes 524320 | tf_op jit(solution)/shard_map/ppermute | solution.py:635
  29.6 0.9 %fusion = bf16[16,8,2048]{2,1,0:T(8,128)(2,1)} fusion(bf16[128,2048]{1,0:T(8,128)(2,1)S(1)} %collective-permute-done.8, bf16[128,2048]{1,0:T(8,128)(2,1)S(1)} %get-tuple-element.39), kind=kLoop, calls=%fused_computation.1 | loop fusion | flops 1048576 | bytes 1572864 | tf_op jit(solution)/shard_map/reshape | solution.py:638
  30.6 4.8 %all-to-all-start = ((bf16[16,8,2048]{2,1,0:T(8,128)(2,1)}), bf16[16,8,2048]{2,1,0:T(8,128)(2,1)S(1)}, u32[]{:S(2)}, u32[]{:S(2)}) async-start(bf16[16,8,2048]{2,1,0:T(8,128)(2,1)} %fusion), calls=%async_computation | async-start | bytes 1048576 | tf_op jit(solution)/shard_map/all_to_all | solution.py:637
  35.4 0.0 copy-done
  35.4 2.9 %collective-permute-start.4 = (f32[1,3,4,512]{3,2,1,0:T(4,128)S(1)}, f32[1,3,4,512]{3,2,1,0:T(4,128)S(1)}, u32[]{:S(2)}, u32[]{:S(2)}) collective-permute-start(f32[1,3,4,512]{3,2,1,0:T(4,128)S(1)} %bitcast.12), channel_id=1, source_target_pairs={{0,16},{4,20},{8,24},{12,28},{16,0},{20,4},{24,8},{28,12},{1,17},{... | collective-permute-start | bytes 73736 | tf_op jit(solution)/shard_map/ppermute | solution.py:632
  38.3 12.8 %collective-permute-done.4.refs_1_ = f32[1,3,4,512]{3,2,1,0:T(4,128)S(1)} collective-permute-done((f32[1,3,4,512]{3,2,1,0:T(4,128)S(1)}, f32[1,3,4,512]{3,2,1,0:T(4,128)S(1)}, u32[]{:S(2)}, u32[]{:S(2)}) %collective-permute-start.4) | collective-permute-done | bytes 24608 | tf_op jit(solution)/shard_map/ppermute | solution.py:632
  51.2 0.1 collective-permute-start.5
  51.3 4.1 %collective-permute-done.5.refs_2_ = f32[2,3,4,512]{3,2,1,0:T(4,128)S(1)} collective-permute-done((f32[2,3,4,512]{3,2,1,0:T(4,128)S(1)}, f32[2,3,4,512]{3,2,1,0:T(4,128)S(1)}, u32[]{:S(2)}, u32[]{:S(2)}) %collective-permute-start.5) | collective-permute-done | bytes 49184 | tf_op jit(solution)/shard_map/ppermute | solution.py:632
  55.4 1.5 %collective-permute-start.6 = (f32[4,3,4,512]{3,2,1,0:T(4,128)S(1)}, f32[4,3,4,512]{3,2,1,0:T(4,128)S(1)}, u32[]{:S(2)}, u32[]{:S(2)}) collective-permute-start(f32[4,3,4,512]{3,2,1,0:T(4,128)S(1)} %pad_maximum_fusion), channel_id=1, source_target_pairs={{0,4},{4,0},{8,12},{12,8},{16,20},{20,16},{24,28},{28,24},{1,5},{5... | collective-permute-start | bytes 294920 | tf_op jit(solution)/shard_map/ppermute | solution.py:632
  56.9 3.2 %collective-permute-done.6.refs_3_ = f32[4,3,4,512]{3,2,1,0:T(4,128)S(1)} collective-permute-done((f32[4,3,4,512]{3,2,1,0:T(4,128)S(1)}, f32[4,3,4,512]{3,2,1,0:T(4,128)S(1)}, u32[]{:S(2)}, u32[]{:S(2)}) %collective-permute-start.6) | collective-permute-done | bytes 98336 | tf_op jit(solution)/shard_map/ppermute | solution.py:632
  60.0 0.0 copy-done.1
  60.0 5.8 %carries.1 = bf16[1024,512]{1,0:T(8,128)(2,1)} custom-call(s32[1]{0:T(128)} %bitcast.place_ref, bf16[1024,512]{1,0:T(8,128)(2,1)} %gate_ref.1, bf16[1024,512]{1,0:T(8,128)(2,1)} %get-tuple-element.22.local_ref, bf16[1024,512]{1,0:T(8,128)(2,1)} %get-tuple-element.23.forward_ref, bf16[1024,512]{1,0:T(8,128)(2,1)} %get-tuple-element.24.backward_ref, ...), custom_call_target="tpu_custom_call" | custom-call | tf_op jit(solution)/shard_map/carries/pallas_call | solution.py:398
  65.8 0.0 all-to-all-done
  65.8 0.9 %combine.1 = bf16[16,2048]{1,0:T(8,128)(2,1)} custom-call(bf16[8,2,8,2048]{3,2,1,0:T(8,128)(2,1)S(1)} %bitcast.11, bf16[2,16,64]{2,1,0:T(8,128)(2,1)S(1)} %get-tuple-element.41.share_ref), custom_call_target="tpu_custom_call" | custom-call | tf_op jit(solution)/shard_map/combine/pallas_call | solution.py:558
  (6 shorter events, 0.1 us)
Async XLA Ops:
  2.8 18.7 %collective-permute-start = (bf16[32,2048]{1,0:T(8,128)(2,1)S(1)}, bf16[32,2048]{1,0:T(8,128)(2,1)S(1)}, u32[]{:S(2)}, u32[]{:S(2)}) collective-permute-start(bf16[32,2048]{1,0:T(8,128)(2,1)S(1)} %get-tuple-element.26), channel_id=1, source_target_pairs={{0,4},{1,21},{4,0},{5,17},{8,12},{9,29},{12,8},{13,25},{16,20},{17... | collective-permute-start | bytes 393224 | tf_op jit(solution)/shard_map/ppermute | solution.py:612
  5.8 15.7 %collective-permute-start.1 = (bf16[32,2048]{1,0:T(8,128)(2,1)S(1)}, bf16[32,2048]{1,0:T(8,128)(2,1)S(1)}, u32[]{:S(2)}, u32[]{:S(2)}) collective-permute-start(bf16[32,2048]{1,0:T(8,128)(2,1)S(1)} %get-tuple-element.27), channel_id=1, source_target_pairs={{0,8},{1,25},{4,12},{5,29},{8,0},{9,17},{12,4},{13,21},{16,24},{17... | collective-permute-start | bytes 393224 | tf_op jit(solution)/shard_map/ppermute | solution.py:612
  7.4 14.2 %collective-permute-start.2 = (bf16[32,2048]{1,0:T(8,128)(2,1)S(1)}, bf16[32,2048]{1,0:T(8,128)(2,1)S(1)}, u32[]{:S(2)}, u32[]{:S(2)}) collective-permute-start(bf16[32,2048]{1,0:T(8,128)(2,1)S(1)} %get-tuple-element.28), channel_id=1, source_target_pairs={{0,12},{1,29},{4,8},{5,25},{8,4},{9,21},{12,0},{13,17},{16,28},{17... | collective-permute-start | bytes 393224 | tf_op jit(solution)/shard_map/ppermute | solution.py:612
  7.4 14.2 %collective-permute-start.3 = (bf16[32,2048]{1,0:T(8,128)(2,1)S(1)}, bf16[32,2048]{1,0:T(8,128)(2,1)S(1)}, u32[]{:S(2)}, u32[]{:S(2)}) collective-permute-start(bf16[32,2048]{1,0:T(8,128)(2,1)S(1)} %get-tuple-element.29), channel_id=1, source_target_pairs={{0,16},{1,1},{4,20},{5,5},{8,24},{9,9},{12,28},{13,13},{16,0},{17,... | collective-permute-start | bytes 393224 | tf_op jit(solution)/shard_map/ppermute | solution.py:612
  21.6 2.0 %collective-permute-start.7 = (bf16[128,2048]{1,0:T(8,128)(2,1)S(1)}, bf16[128,2048]{1,0:T(8,128)(2,1)S(1)}, u32[]{:S(2)}, u32[]{:S(2)}) collective-permute-start(bf16[128,2048]{1,0:T(8,128)(2,1)S(1)} %constant_dynamic-update-slice_fusion.own_ref), channel_id=1, source_target_pairs={{0,1},{1,0},{2,3},{3,2},{4,5},{5,4},{6,7},{7,6},{8,9},{9,8},{10,11... | collective-permute-start | bytes 1572872 | tf_op jit(solution)/shard_map/ppermute | solution.py:627
  23.6 11.8 %copy-start = (f32[3,4,512]{2,1,0:T(4,128)S(1)}, f32[3,4,512]{2,1,0:T(4,128)}, u32[]{:S(2)}) copy-start(f32[3,4,512]{2,1,0:T(4,128)} %get-tuple-element.31) | copy-start | bytes 73732
  23.6 36.4 %copy-start.1 = (f32[4,8,512]{2,1,0:T(8,128)S(1)}, f32[4,8,512]{2,1,0:T(8,128)}, u32[]{:S(2)}) copy-start(f32[4,8,512]{2,1,0:T(8,128)} %get-tuple-element.25.chunk_ref) | copy-start | bytes 196612
  27.7 2.0 %collective-permute-start.8 = (bf16[128,2048]{1,0:T(8,128)(2,1)S(1)}, bf16[128,2048]{1,0:T(8,128)(2,1)S(1)}, u32[]{:S(2)}, u32[]{:S(2)}) collective-permute-start(bf16[128,2048]{1,0:T(8,128)(2,1)S(1)} %get-tuple-element.40), channel_id=1, source_target_pairs={{0,1},{1,0},{2,3},{3,2},{4,5},{5,4},{6,7},{7,6},{8,9},{9,8},{10,11... | collective-permute-start | bytes 1572872 | tf_op jit(solution)/shard_map/ppermute | solution.py:635
  30.6 35.3 %all-to-all-start = ((bf16[16,8,2048]{2,1,0:T(8,128)(2,1)}), bf16[16,8,2048]{2,1,0:T(8,128)(2,1)S(1)}, u32[]{:S(2)}, u32[]{:S(2)}) async-start(bf16[16,8,2048]{2,1,0:T(8,128)(2,1)} %fusion), calls=%async_computation | async-start | bytes 1048576 | tf_op jit(solution)/shard_map/all_to_all | solution.py:637
  35.4 15.7 %collective-permute-start.4 = (f32[1,3,4,512]{3,2,1,0:T(4,128)S(1)}, f32[1,3,4,512]{3,2,1,0:T(4,128)S(1)}, u32[]{:S(2)}, u32[]{:S(2)}) collective-permute-start(f32[1,3,4,512]{3,2,1,0:T(4,128)S(1)} %bitcast.12), channel_id=1, source_target_pairs={{0,16},{4,20},{8,24},{12,28},{16,0},{20,4},{24,8},{28,12},{1,17},{... | collective-permute-start | bytes 73736 | tf_op jit(solution)/shard_map/ppermute | solution.py:632
  51.2 4.2 %collective-permute-start.5 = (f32[2,3,4,512]{3,2,1,0:T(4,128)S(1)}, f32[2,3,4,512]{3,2,1,0:T(4,128)S(1)}, u32[]{:S(2)}, u32[]{:S(2)}) collective-permute-start(f32[2,3,4,512]{3,2,1,0:T(4,128)S(1)} %pad_maximum_fusion.1), channel_id=1, source_target_pairs={{0,8},{4,12},{8,0},{12,4},{16,24},{20,28},{24,16},{28,20},{1,9},{5... | collective-permute-start | bytes 147464 | tf_op jit(solution)/shard_map/ppermute | solution.py:632
  55.4 4.7 %collective-permute-start.6 = (f32[4,3,4,512]{3,2,1,0:T(4,128)S(1)}, f32[4,3,4,512]{3,2,1,0:T(4,128)S(1)}, u32[]{:S(2)}, u32[]{:S(2)}) collective-permute-start(f32[4,3,4,512]{3,2,1,0:T(4,128)S(1)} %pad_maximum_fusion), channel_id=1, source_target_pairs={{0,4},{4,0},{8,12},{12,8},{16,20},{20,16},{24,28},{28,24},{1,5},{5... | collective-permute-start | bytes 294920 | tf_op jit(solution)/shard_map/ppermute | solution.py:632

commit v3 on v2

--- a/solution.py
+++ b/solution.py
@@ -265,7 +265,6 @@
 
 
 def carry_kernel(
-    place_ref,
     gate_ref,
     local_ref,
     forward_ref,
@@ -282,7 +281,7 @@
     per = length // CHUNKS
     pitch = per + 4
     f32 = jnp.float32
-    place = place_ref[0]
+    place = lax.axis_index("ep")
     count = all_ref.shape[1]
     away, bit = [0], count // 2
     for i, piece in enumerate(pieces):
@@ -390,44 +389,42 @@
     lax.fori_loop(0, length // span, finish, 0)
 
 
-def add_carries(place, gate, arrays, local, forward, backward, chunks, everyone):
+def add_carries(gate, arrays, local, forward, backward, chunks, everyone):
     taps, decay_w, input_w, rate = arrays
     length, channels = local.shape
     count = sum(piece.shape[0] for piece in everyone)
-    col = lambda h, p: (0, h)
+    col = lambda h: (0, h)
     return pl.pallas_call(
         carry_kernel,
-        grid_spec=pltpu.PrefetchScalarGridSpec(
-            num_scalar_prefetch=1,
-            grid=(channels // LANES,),
-            in_specs=[pl.BlockSpec((length, LANES), col)] * 4
+        grid=(channels // LANES,),
+        in_specs=[pl.BlockSpec((length, LANES), col)] * 4
             + [
-                pl.BlockSpec((4, CHUNKS, LANES), lambda h, p: (0, 0, h)),
+                pl.BlockSpec((4, CHUNKS, LANES), lambda h: (0, 0, h)),
                 pl.BlockSpec((4, LANES), col),
-                pl.BlockSpec((2, 1, LANES, LANES), lambda h, p: (0, h, 0, 0)),
-                pl.BlockSpec((2, 1, LANES, LANES), lambda h, p: (0, h, 0, 0)),
+                pl.BlockSpec((2, 1, LANES, LANES), lambda h: (0, h, 0, 0)),
+                pl.BlockSpec((2, 1, LANES, LANES), lambda h: (0, h, 0, 0)),
                 pl.BlockSpec((2, LANES), col),
             ]
-            + [pl.BlockSpec((len(piece), 3, 4, LANES), lambda h, p: (0, 0, 0, h)) for piece in everyone],
-            out_specs=pl.BlockSpec((length, LANES), col),
-            scratch_shapes=[
-                pltpu.VMEM((12, count, LANES), jnp.float32),
-                pltpu.VMEM((2, CHUNKS, LANES), jnp.float32),
-                pltpu.VMEM((length + 4 * CHUNKS, LANES), jnp.float32),
-            ],
-        ),
+            + [pl.BlockSpec((len(piece), 3, 4, LANES), lambda h: (0, 0, 0, h)) for piece in everyone],
+        out_specs=pl.BlockSpec((length, LANES), col),
+        scratch_shapes=[
+            pltpu.VMEM((12, count, LANES), jnp.float32),
+            pltpu.VMEM((2, CHUNKS, LANES), jnp.float32),
+            pltpu.VMEM((length + 4 * CHUNKS, LANES), jnp.float32),
+        ],
         out_shape=jax.ShapeDtypeStruct((length, channels), jnp.bfloat16),
         compiler_params=pltpu.CompilerParams(vmem_limit_bytes=20 << 20),
         name="carries",
     )(
-        place, far(gate), far(local), far(forward), far(backward), chunks,
+        far(gate), far(local), far(forward), far(backward), chunks,
         far(taps), far(decay_w), far(input_w), far(rate), *everyone
     )
 
 
 def prepare_kernel(
-    ids_ref, in_ref, gain_ref, routes_ref, scores_ref, share_ref, *send_refs, block_rows, experts, capacity, cores
+    in_ref, gain_ref, routes_ref, scores_ref, share_ref, *send_refs, block_rows, experts, capacity, cores
 ):
+    place, plane, core = [lax.axis_index(name) for name in ("ep", "plane", "core")]
     f32, bf16 = jnp.float32, jnp.bfloat16
     rows = in_ref.shape[0]
     wide = in_ref[...].astype(f32)
@@ -454,7 +451,7 @@
     low = (held - high.astype(f32)).astype(bf16)
     row = lax.broadcasted_iota(jnp.int32, (block_rows, rows), 0)
     col = lax.broadcasted_iota(jnp.int32, (block_rows, rows), 1)
-    own = (col == row + ids_ref[1] * block_rows).astype(f32).astype(bf16)
+    own = (col == row + (plane * cores + core) * block_rows).astype(f32).astype(bf16)
     for i, part in enumerate((high, low)):
         share_ref[i] = lax.dot_general(
             own, part, (((1,), (1,)), ((), ())), preferred_element_type=f32
@@ -467,44 +464,41 @@
     token = lax.broadcasted_iota(jnp.int32, (width, rows), 1)
     planes = blocks // cores
     block = ((slot // capacity) % planes) * cores + (slot // (capacity * planes)) % cores
-    distance = (slot // each + 1 + ids_ref[0] * (experts // cores)) % experts
-    pick = placed(distance ^ ids_ref[2], slot % capacity)
+    distance = (slot // each + 1 + core * (experts // cores)) % experts
+    pick = placed(distance ^ place, slot % capacity)
     pick = jnp.where(token // block_rows == block, pick, 0.0).astype(bf16)
     send = jnp.dot(pick, normed, preferred_element_type=f32).astype(bf16)
     for d in range(experts // cores):
         send_refs[d][...] = send[d * each : (d + 1) * each]
 
 
-def prepare(ids, expert_in, gain, routes, scores, block_rows, experts, capacity, cores):
+def prepare(expert_in, gain, routes, scores, block_rows, experts, capacity, cores):
     rows, model = expert_in.shape
     slots = experts * capacity
     each = rows // block_rows * capacity
-    whole = lambda *shape: pl.BlockSpec(shape, lambda i, c: (0,) * len(shape))
+    whole = lambda *shape: pl.BlockSpec(shape, lambda i: (0,) * len(shape))
     return pl.pallas_call(
         functools.partial(
             prepare_kernel, block_rows=block_rows, experts=experts, capacity=capacity, cores=cores
         ),
-        grid_spec=pltpu.PrefetchScalarGridSpec(
-            num_scalar_prefetch=1,
-            grid=(1,),
-            in_specs=[whole(rows, model), whole(1, model), whole(TOP_K, rows), whole(TOP_K, rows)],
-            out_specs=[whole(2, block_rows, slots)] + [whole(each, model)] * (experts // cores),
-        ),
+        grid=(1,),
+        in_specs=[whole(rows, model), whole(1, model), whole(TOP_K, rows), whole(TOP_K, rows)],
+        out_specs=[whole(2, block_rows, slots)] + [whole(each, model)] * (experts // cores),
         out_shape=[
             jax.ShapeDtypeStruct((2, block_rows, slots), jnp.bfloat16),
         ]
         + [jax.ShapeDtypeStruct((each, model), jnp.bfloat16)] * (experts // cores),
         compiler_params=pltpu.CompilerParams(vmem_limit_bytes=24 << 20),
         name="prepare",
-    )(ids, far(expert_in), far(gain.reshape(1, model)), far(routes.T), far(scores.T))
-
-
-def expert_kernel(groups, cores, ids_ref, own_ref, other_ref, gate_ref, up_ref, down_ref, keep_ref, send_ref, rows_ref, hidden_ref):
+    )(far(expert_in), far(gain.reshape(1, model)), far(routes.T), far(scores.T))
+
+
+def expert_kernel(groups, cores, own_ref, other_ref, gate_ref, up_ref, down_ref, keep_ref, send_ref, rows_ref, hidden_ref):
     f32, bf16 = jnp.float32, jnp.bfloat16
     half, model = own_ref.shape
     hidden = gate_ref.shape[1]
     wide, tall = math.gcd(hidden, 256), math.gcd(model, 256)
-    core, place = ids_ref[0], ids_ref[2]
+    core, place = lax.axis_index("core"), lax.axis_index("ep")
     count = groups // cores
     each = half // groups
     for s, ref in enumerate((own_ref, other_ref)):
@@ -526,20 +520,20 @@
         send_ref[:, n : n + tall] = out[half:]
 
 
-def expert(ids, groups, cores, own, other, gate_weight, up_weight, down_weight):
+def expert(groups, cores, own, other, gate_weight, up_weight, down_weight):
     half, model = own.shape
     hidden = gate_weight.shape[1]
     bf16 = jnp.bfloat16
     vmem = pl.BlockSpec(memory_space=pltpu.VMEM)
     return pl.pallas_call(
         functools.partial(expert_kernel, groups, cores),
-        in_specs=[pl.BlockSpec(memory_space=pltpu.SMEM)] + [vmem] * 5,
+        in_specs=[vmem] * 5,
         out_specs=[vmem, vmem],
         out_shape=[jax.ShapeDtypeStruct((half, model), bf16)] * 2,
         scratch_shapes=[pltpu.VMEM((2 * half, model), bf16), pltpu.VMEM((2 * half, hidden), bf16)],
         compiler_params=pltpu.CompilerParams(vmem_limit_bytes=20 << 20),
         name="experts",
-    )(ids, own, other, gate_weight, up_weight, down_weight)
+    )(own, other, gate_weight, up_weight, down_weight)
 
 
 def combine_kernel(back_ref, share_ref, out_ref):
@@ -582,18 +576,13 @@
     experts = lax.axis_size("ep")
     planes = lax.axis_size("plane")
     cores = lax.axis_size("core")
-    place = lax.axis_index("ep")
-    core = lax.axis_index("core")
-    block = lax.axis_index("plane") * cores + core
     group_rows, model = expert_in.shape
     block_rows = group_rows // (planes * cores)
     capacity = max(2, 2 * block_rows * TOP_K // experts)
 
     swap = [(i, cores - 1 - i) for i in range(cores)]
     far_by = lambda d: [(i, i ^ d) for i in range(experts)]
-    ids = jnp.stack([core, block, place]).astype(jnp.int32)
     share, *outgoing = prepare(
-        ids,
         expert_in,
         norm_gain,
         routes,
@@ -631,14 +620,14 @@
         held = everyone[0] if len(everyone) == 1 else jnp.concatenate(everyone, axis=0)
         everyone.append(lax.ppermute(held, "ep", far_by(bit)))
         bit //= 2
-    keep, send = expert(ids, experts, cores, arrived, other, *weights)
+    keep, send = expert(experts, cores, arrived, other, *weights)
     theirs = lax.ppermute(send, "core", swap)
     keep = (keep.astype(jnp.float32) + theirs.astype(jnp.float32)).astype(jnp.bfloat16)
     back = lax.all_to_all(
         keep.reshape(experts * planes, capacity, model), ("ep", "plane"), 0, 0, tiled=True
     ).reshape(experts, planes, capacity, model)
     recurrent_out = add_carries(
-        place.reshape(1).astype(jnp.int32), gate_path, arrays[1:5], mixed, forward, backward, chunks, everyone
+        gate_path, arrays[1:5], mixed, forward, backward, chunks, everyone
     )
     expert_out = combine(back, share)
     return (recurrent_out, expert_out)

time: 67.1 us -> 66 us (0.984)
  Pallas kernels: 22 us -> 20.9 us
  transfers between devices with their start and end apart: 10 -> 10, of which waited for: 5 -> 5; matrix products, arithmetic and copies ran while one was open for 0% -> 0% of each run, Pallas kernels for 22% -> 23%
where the time goes in v3:
time: 66 us; the launch traced here: 65.6 us
  waiting for transfers between devices  23.8 us (36%)
  Pallas kernels  20.9 us (32%)
  starting transfers between devices  19.1 us (29%)
  other arithmetic  0.97 us (1%)
  between operations  0.78 us (1%)
    ppermute x3, waiting for transfers between devices, local(): everyone.append(lax.ppermute(held, 'ep', far_by(bit)))  20.1 us
    ppermute x4, starting transfers between devices, local(): arrived.append(lax.ppermute(rows, ('ep', 'core'), pairs))  9.51 us
    pallas_call x1, Pallas kernels, local_recurrence(): pl.pallas_call(functools.partial(gates_kernel, first, count, len(weights)...  9.21 us
    pallas_call x1, Pallas kernels, add_carries(): pl.pallas_call(carry_kernel, grid=(channels // LANES,), in_specs=[pl.Bloc...  5.8 us
    all_to_all x1, starting transfers between devices, local(): lax.all_to_all(keep.reshape(experts * planes, capacity, model), ('ep', 'p...  4.84 us
    ppermute x3, starting transfers between devices, local(): everyone.append(lax.ppermute(held, 'ep', far_by(bit)))  4.49 us
    pallas_call x1, Pallas kernels, expert(): pl.pallas_call(functools.partial(expert_kernel, groups, cores), in_specs=...  3.5 us
    ppermute x1, waiting for transfers between devices, local(): other = lax.ppermute(arrived, 'core', swap)  1.9 us
  transfers between devices with their start and end apart: 10, of which 5 were waited for; matrix products, arithmetic and copies ran while one was open for 0% of the time, Pallas kernels for 23%

profile of v3, /device:TPU:0, one launch (start us, length us, event | category | flops | bytes accessed | tf_op | source)
XLA Modules:
  0.0 65.6 jit_solution(8046409936940980211)
XLA Ops:
  0.6 1.5 %prepare.1 = (bf16[2,16,64]{2,1,0:T(8,128)(2,1)S(1)}, bf16[32,2048]{1,0:T(8,128)(2,1)S(1)}, bf16[32,2048]{1,0:T(8,128)(2,1)S(1)}, bf16[32,2048]{1,0:T(8,128)(2,1)S(1)}, bf16[32,2048]{1,0:T(8,128)(2,1)S(1)}) custom-call(bf16[64,2048]{1,0:T(8,128)(2,1)} %in_ref.1, f32[1,2048]{1,0:T(1,128)} %bitcast.14, s32[2,64]{1,0:T(2,128)} %bitcast.15, f32[2,64]{1,0:T(2,128)} %bitcast.16), custom_call_target="tpu_custom_call" | custom-call | tf_op jit(solution)/shard_map/prepare/pallas_call | solution.py:480
  2.2 3.0 %collective-permute-start = (bf16[32,2048]{1,0:T(8,128)(2,1)S(1)}, bf16[32,2048]{1,0:T(8,128)(2,1)S(1)}, u32[]{:S(2)}, u32[]{:S(2)}) collective-permute-start(bf16[32,2048]{1,0:T(8,128)(2,1)S(1)} %get-tuple-element.26), channel_id=1, source_target_pairs={{0,4},{1,21},{4,0},{5,17},{8,12},{9,29},{12,8},{13,25},{16,20},{17... | collective-permute-start | bytes 393224 | tf_op jit(solution)/shard_map/ppermute | solution.py:601
  5.2 1.6 %collective-permute-start.1 = (bf16[32,2048]{1,0:T(8,128)(2,1)S(1)}, bf16[32,2048]{1,0:T(8,128)(2,1)S(1)}, u32[]{:S(2)}, u32[]{:S(2)}) collective-permute-start(bf16[32,2048]{1,0:T(8,128)(2,1)S(1)} %get-tuple-element.27), channel_id=1, source_target_pairs={{0,8},{1,25},{4,12},{5,29},{8,0},{9,17},{12,4},{13,21},{16,24},{17... | collective-permute-start | bytes 393224 | tf_op jit(solution)/shard_map/ppermute | solution.py:601
  6.8 0.0 collective-permute-start.2
  6.8 4.9 %collective-permute-start.3 = (bf16[32,2048]{1,0:T(8,128)(2,1)S(1)}, bf16[32,2048]{1,0:T(8,128)(2,1)S(1)}, u32[]{:S(2)}, u32[]{:S(2)}) collective-permute-start(bf16[32,2048]{1,0:T(8,128)(2,1)S(1)} %get-tuple-element.29), channel_id=1, source_target_pairs={{0,16},{1,1},{4,20},{5,5},{8,24},{9,9},{12,28},{13,13},{16,0},{17,... | collective-permute-start | bytes 393224 | tf_op jit(solution)/shard_map/ppermute | solution.py:601
  11.7 9.2 %recurrence.1 = (bf16[1024,512]{1,0:T(8,128)(2,1)}, bf16[1024,512]{1,0:T(8,128)(2,1)}, bf16[1024,512]{1,0:T(8,128)(2,1)}, f32[4,8,512]{2,1,0:T(8,128)}, f32[3,4,...) custom-call(bf16[1024,512]{1,0:T(8,128)(2,1)} %refs_0_.1, ...), custom_call_target="tpu_custom_call" | custom-call | tf_op jit(solution)/shard_map/recurrence/pallas_call | solution.py:222
  20.9 0.0 collective-permute-done
  20.9 0.0 collective-permute-done.1
  20.9 0.0 collective-permute-done.2
  20.9 0.0 collective-permute-done.3
  21.0 0.1 collective-permute-start.7
  21.1 1.9 %collective-permute-done.7.other_ref = bf16[128,2048]{1,0:T(8,128)(2,1)S(1)} collective-permute-done((bf16[128,2048]{1,0:T(8,128)(2,1)S(1)}, bf16[128,2048]{1,0:T(8,128)(2,1)S(1)}, u32[]{:S(2)}, u32[]{:S(2)}) %collective-permute-start.7) | collective-permute-done | bytes 524320 | tf_op jit(solution)/shard_map/ppermute | solution.py:616
  23.0 0.0 copy-start
  23.0 0.0 copy-start.1
  23.0 3.5 %experts.1 = (bf16[128,2048]{1,0:T(8,128)(2,1)S(1)}, bf16[128,2048]{1,0:T(8,128)(2,1)S(1)}) custom-call(bf16[128,2048]{1,0:T(8,128)(2,1)S(1)} %constant_dynamic-update-slice_fusion.own_ref, bf16[128,2048]{1,0:T(8,128)(2,1)S(1)} %collective-permute-done.7.other_ref, bf16[2048,1024]{1,0:T(8,128)(2,1)S(1)} %get-tuple-element.36.gate_ref, ...), custom_call_target="tpu_custom_call" | custom-call | tf_op jit(solution)/shard_map/experts/pallas_call | solution.py:528
  26.5 0.2 collective-permute-start.8
  26.7 1.8 %collective-permute-done.8 = bf16[128,2048]{1,0:T(8,128)(2,1)S(1)} collective-permute-done((bf16[128,2048]{1,0:T(8,128)(2,1)S(1)}, bf16[128,2048]{1,0:T(8,128)(2,1)S(1)}, u32[]{:S(2)}, u32[]{:S(2)}) %collective-permute-start.8) | collective-permute-done | bytes 524320 | tf_op jit(solution)/shard_map/ppermute | solution.py:624
  28.5 0.9 %fusion = bf16[16,8,2048]{2,1,0:T(8,128)(2,1)} fusion(bf16[128,2048]{1,0:T(8,128)(2,1)S(1)} %collective-permute-done.8, bf16[128,2048]{1,0:T(8,128)(2,1)S(1)} %get-tuple-element.39), kind=kLoop, calls=%fused_computation.1 | loop fusion | flops 1048576 | bytes 1572864 | tf_op jit(solution)/shard_map/reshape | solution.py:627
  29.4 4.8 %all-to-all-start = ((bf16[16,8,2048]{2,1,0:T(8,128)(2,1)}), bf16[16,8,2048]{2,1,0:T(8,128)(2,1)S(1)}, u32[]{:S(2)}, u32[]{:S(2)}) async-start(bf16[16,8,2048]{2,1,0:T(8,128)(2,1)} %fusion), calls=%async_computation | async-start | bytes 1048576 | tf_op jit(solution)/shard_map/all_to_all | solution.py:626
  34.3 0.0 copy-done
  34.3 2.9 %collective-permute-start.4 = (f32[1,3,4,512]{3,2,1,0:T(4,128)S(1)}, f32[1,3,4,512]{3,2,1,0:T(4,128)S(1)}, u32[]{:S(2)}, u32[]{:S(2)}) collective-permute-start(f32[1,3,4,512]{3,2,1,0:T(4,128)S(1)} %bitcast.9), channel_id=1, source_target_pairs={{0,16},{4,20},{8,24},{12,28},{16,0},{20,4},{24,8},{28,12},{1,17},{... | collective-permute-start | bytes 73736 | tf_op jit(solution)/shard_map/ppermute | solution.py:621
  37.2 12.8 %collective-permute-done.4.refs_1_ = f32[1,3,4,512]{3,2,1,0:T(4,128)S(1)} collective-permute-done((f32[1,3,4,512]{3,2,1,0:T(4,128)S(1)}, f32[1,3,4,512]{3,2,1,0:T(4,128)S(1)}, u32[]{:S(2)}, u32[]{:S(2)}) %collective-permute-start.4) | collective-permute-done | bytes 24608 | tf_op jit(solution)/shard_map/ppermute | solution.py:621
  50.0 0.1 collective-permute-start.5
  50.1 4.1 %collective-permute-done.5.refs_2_ = f32[2,3,4,512]{3,2,1,0:T(4,128)S(1)} collective-permute-done((f32[2,3,4,512]{3,2,1,0:T(4,128)S(1)}, f32[2,3,4,512]{3,2,1,0:T(4,128)S(1)}, u32[]{:S(2)}, u32[]{:S(2)}) %collective-permute-start.5) | collective-permute-done | bytes 49184 | tf_op jit(solution)/shard_map/ppermute | solution.py:621
  54.2 1.5 %collective-permute-start.6 = (f32[4,3,4,512]{3,2,1,0:T(4,128)S(1)}, f32[4,3,4,512]{3,2,1,0:T(4,128)S(1)}, u32[]{:S(2)}, u32[]{:S(2)}) collective-permute-start(f32[4,3,4,512]{3,2,1,0:T(4,128)S(1)} %pad_maximum_fusion), channel_id=1, source_target_pairs={{0,4},{4,0},{8,12},{12,8},{16,20},{20,16},{24,28},{28,24},{1,5},{5... | collective-permute-start | bytes 294920 | tf_op jit(solution)/shard_map/ppermute | solution.py:621
  55.7 3.2 %collective-permute-done.6.refs_3_ = f32[4,3,4,512]{3,2,1,0:T(4,128)S(1)} collective-permute-done((f32[4,3,4,512]{3,2,1,0:T(4,128)S(1)}, f32[4,3,4,512]{3,2,1,0:T(4,128)S(1)}, u32[]{:S(2)}, u32[]{:S(2)}) %collective-permute-start.6) | collective-permute-done | bytes 98336 | tf_op jit(solution)/shard_map/ppermute | solution.py:621
  58.9 0.0 copy-done.1
  58.9 5.8 %carries.1 = bf16[1024,512]{1,0:T(8,128)(2,1)} custom-call(bf16[1024,512]{1,0:T(8,128)(2,1)} %gate_ref.1, bf16[1024,512]{1,0:T(8,128)(2,1)} %get-tuple-element.22.local_ref, bf16[1024,512]{1,0:T(8,128)(2,1)} %get-tuple-element.23.forward_ref, bf16[1024,512]{1,0:T(8,128)(2,1)} %get-tuple-element.24.backward_ref, f32[4,8,512]{2,1,0:T(8,128)S(1)} %copy-done.1, ...), custom_call_target="tpu_custom_call" | custom-call | tf_op jit(solution)/shard_map/carries/pallas_call | solution.py:397
  64.7 0.0 all-to-all-done
  64.7 0.9 %combine.1 = bf16[16,2048]{1,0:T(8,128)(2,1)} custom-call(bf16[8,2,8,2048]{3,2,1,0:T(8,128)(2,1)S(1)} %bitcast.8, bf16[2,16,64]{2,1,0:T(8,128)(2,1)S(1)} %get-tuple-element.41.share_ref), custom_call_target="tpu_custom_call" | custom-call | tf_op jit(solution)/shard_map/combine/pallas_call | solution.py:552
  (6 shorter events, 0.1 us)
Async XLA Ops:
  2.2 18.7 %collective-permute-start = (bf16[32,2048]{1,0:T(8,128)(2,1)S(1)}, bf16[32,2048]{1,0:T(8,128)(2,1)S(1)}, u32[]{:S(2)}, u32[]{:S(2)}) collective-permute-start(bf16[32,2048]{1,0:T(8,128)(2,1)S(1)} %get-tuple-element.26), channel_id=1, source_target_pairs={{0,4},{1,21},{4,0},{5,17},{8,12},{9,29},{12,8},{13,25},{16,20},{17... | collective-permute-start | bytes 393224 | tf_op jit(solution)/shard_map/ppermute | solution.py:601
  5.2 15.7 %collective-permute-start.1 = (bf16[32,2048]{1,0:T(8,128)(2,1)S(1)}, bf16[32,2048]{1,0:T(8,128)(2,1)S(1)}, u32[]{:S(2)}, u32[]{:S(2)}) collective-permute-start(bf16[32,2048]{1,0:T(8,128)(2,1)S(1)} %get-tuple-element.27), channel_id=1, source_target_pairs={{0,8},{1,25},{4,12},{5,29},{8,0},{9,17},{12,4},{13,21},{16,24},{17... | collective-permute-start | bytes 393224 | tf_op jit(solution)/shard_map/ppermute | solution.py:601
  6.8 14.2 %collective-permute-start.2 = (bf16[32,2048]{1,0:T(8,128)(2,1)S(1)}, bf16[32,2048]{1,0:T(8,128)(2,1)S(1)}, u32[]{:S(2)}, u32[]{:S(2)}) collective-permute-start(bf16[32,2048]{1,0:T(8,128)(2,1)S(1)} %get-tuple-element.28), channel_id=1, source_target_pairs={{0,12},{1,29},{4,8},{5,25},{8,4},{9,21},{12,0},{13,17},{16,28},{17... | collective-permute-start | bytes 393224 | tf_op jit(solution)/shard_map/ppermute | solution.py:601
  6.8 14.2 %collective-permute-start.3 = (bf16[32,2048]{1,0:T(8,128)(2,1)S(1)}, bf16[32,2048]{1,0:T(8,128)(2,1)S(1)}, u32[]{:S(2)}, u32[]{:S(2)}) collective-permute-start(bf16[32,2048]{1,0:T(8,128)(2,1)S(1)} %get-tuple-element.29), channel_id=1, source_target_pairs={{0,16},{1,1},{4,20},{5,5},{8,24},{9,9},{12,28},{13,13},{16,0},{17,... | collective-permute-start | bytes 393224 | tf_op jit(solution)/shard_map/ppermute | solution.py:601
  21.0 2.0 %collective-permute-start.7 = (bf16[128,2048]{1,0:T(8,128)(2,1)S(1)}, bf16[128,2048]{1,0:T(8,128)(2,1)S(1)}, u32[]{:S(2)}, u32[]{:S(2)}) collective-permute-start(bf16[128,2048]{1,0:T(8,128)(2,1)S(1)} %constant_dynamic-update-slice_fusion.own_ref), channel_id=1, source_target_pairs={{0,1},{1,0},{2,3},{3,2},{4,5},{5,4},{6,7},{7,6},{8,9},{9,8},{10,11... | collective-permute-start | bytes 1572872 | tf_op jit(solution)/shard_map/ppermute | solution.py:616
  23.0 11.3 %copy-start = (f32[3,4,512]{2,1,0:T(4,128)S(1)}, f32[3,4,512]{2,1,0:T(4,128)}, u32[]{:S(2)}) copy-start(f32[3,4,512]{2,1,0:T(4,128)} %get-tuple-element.31) | copy-start | bytes 73732
  23.0 35.9 %copy-start.1 = (f32[4,8,512]{2,1,0:T(8,128)S(1)}, f32[4,8,512]{2,1,0:T(8,128)}, u32[]{:S(2)}) copy-start(f32[4,8,512]{2,1,0:T(8,128)} %get-tuple-element.25.chunk_ref) | copy-start | bytes 196612
  26.5 2.0 %collective-permute-start.8 = (bf16[128,2048]{1,0:T(8,128)(2,1)S(1)}, bf16[128,2048]{1,0:T(8,128)(2,1)S(1)}, u32[]{:S(2)}, u32[]{:S(2)}) collective-permute-start(bf16[128,2048]{1,0:T(8,128)(2,1)S(1)} %get-tuple-element.40), channel_id=1, source_target_pairs={{0,1},{1,0},{2,3},{3,2},{4,5},{5,4},{6,7},{7,6},{8,9},{9,8},{10,11... | collective-permute-start | bytes 1572872 | tf_op jit(solution)/shard_map/ppermute | solution.py:624
  29.4 35.3 %all-to-all-start = ((bf16[16,8,2048]{2,1,0:T(8,128)(2,1)}), bf16[16,8,2048]{2,1,0:T(8,128)(2,1)S(1)}, u32[]{:S(2)}, u32[]{:S(2)}) async-start(bf16[16,8,2048]{2,1,0:T(8,128)(2,1)} %fusion), calls=%async_computation | async-start | bytes 1048576 | tf_op jit(solution)/shard_map/all_to_all | solution.py:626
  34.3 15.7 %collective-permute-start.4 = (f32[1,3,4,512]{3,2,1,0:T(4,128)S(1)}, f32[1,3,4,512]{3,2,1,0:T(4,128)S(1)}, u32[]{:S(2)}, u32[]{:S(2)}) collective-permute-start(f32[1,3,4,512]{3,2,1,0:T(4,128)S(1)} %bitcast.9), channel_id=1, source_target_pairs={{0,16},{4,20},{8,24},{12,28},{16,0},{20,4},{24,8},{28,12},{1,17},{... | collective-permute-start | bytes 73736 | tf_op jit(solution)/shard_map/ppermute | solution.py:621
  50.0 4.2 %collective-permute-start.5 = (f32[2,3,4,512]{3,2,1,0:T(4,128)S(1)}, f32[2,3,4,512]{3,2,1,0:T(4,128)S(1)}, u32[]{:S(2)}, u32[]{:S(2)}) collective-permute-start(f32[2,3,4,512]{3,2,1,0:T(4,128)S(1)} %pad_maximum_fusion.1), channel_id=1, source_target_pairs={{0,8},{4,12},{8,0},{12,4},{16,24},{20,28},{24,16},{28,20},{1,9},{5... | collective-permute-start | bytes 147464 | tf_op jit(solution)/shard_map/ppermute | solution.py:621
  54.2 4.7 %collective-permute-start.6 = (f32[4,3,4,512]{3,2,1,0:T(4,128)S(1)}, f32[4,3,4,512]{3,2,1,0:T(4,128)S(1)}, u32[]{:S(2)}, u32[]{:S(2)}) collective-permute-start(f32[4,3,4,512]{3,2,1,0:T(4,128)S(1)} %pad_maximum_fusion), channel_id=1, source_target_pairs={{0,4},{4,0},{8,12},{12,8},{16,20},{20,16},{24,28},{28,24},{1,5},{5... | collective-permute-start | bytes 294920 | tf_op jit(solution)/shard_map/ppermute | solution.py:621

commit v4 on v3

--- a/solution.py
+++ b/solution.py
@@ -63,6 +63,7 @@
     pitch = per + 4
     f32 = jnp.float32
 
+    lanes = pl.ds(pl.multiple_of((pl.program_id(0) + first) * LANES, LANES), LANES)
     step = pl.program_id(0)
 
     def fetch(h):
@@ -136,7 +137,7 @@
                     state_ref[pl.ds(start + i * CHUNKS, CHUNKS), :] = state
                     if i % 2:
                         two = pl.ds(start + (i - 1) * CHUNKS, 2 * CHUNKS)
-                        forward_ref[two, :] = jnp.concatenate([held[1], prod]).astype(forward_ref.dtype)
+                        forward_ref[two, lanes] = jnp.concatenate([held[1], prod]).astype(forward_ref.dtype)
             else:
                 decay_ref[pl.ds(start, size), :] = decay
                 drive_ref[pl.ds(start, size), :] = drive
@@ -167,8 +168,8 @@
                 last_total, last_prod = total, prod
             else:
                 two = pl.ds(start + i * CHUNKS, 2 * CHUNKS)
-                local_ref[two, :] = jnp.concatenate([total, last_total]).astype(local_ref.dtype)
-                backward_ref[two, :] = jnp.concatenate([prod, last_prod]).astype(backward_ref.dtype)
+                local_ref[two, lanes] = jnp.concatenate([total, last_total]).astype(local_ref.dtype)
+                backward_ref[two, lanes] = jnp.concatenate([prod, last_prod]).astype(backward_ref.dtype)
         return state, prod
 
     backward_end, backward_prod = lax.fori_loop(0, blocks, back, (zero, one))
@@ -232,17 +233,17 @@
         ]
         + [any_ref] * (len(weights) + len(partial)),
         out_specs=[
-            pl.BlockSpec((length, LANES), col),
-            pl.BlockSpec((length, LANES), col),
-            pl.BlockSpec((length, LANES), col),
+            pl.BlockSpec(memory_space=pltpu.VMEM),
+            pl.BlockSpec(memory_space=pltpu.VMEM),
+            pl.BlockSpec(memory_space=pltpu.VMEM),
             pl.BlockSpec((4, CHUNKS, LANES), lambda h: (0, 0, h + first)),
             pl.BlockSpec((3, 4, LANES), lambda h: (0, 0, h + first)),
         ]
         + [pl.BlockSpec(memory_space=pltpu.VMEM)] * len(weights),
         out_shape=[
-            pltpu.HBM((length, channels), bf16),
-            pltpu.HBM((length, channels), bf16),
-            pltpu.HBM((length, channels), bf16),
+            pltpu.VMEM((length, channels), bf16),
+            pltpu.VMEM((length, channels), bf16),
+            pltpu.VMEM((length, channels), bf16),
             pltpu.HBM((4, CHUNKS, channels), f32),
             pltpu.HBM((3, 4, channels), f32),
         ]

time: 66 us -> 65.3 us (0.989)
  Pallas kernels: 20.9 us -> 20.2 us
    pallas_call x1, Pallas kernels: 9.21 us -> 8.53 us  [local_recurrence(): pl.pallas_call(functools.partial(gates_kernel, first, count, len(weights)...]
  transfers between devices with their start and end apart: 10 -> 10, of which waited for: 5 -> 5; matrix products, arithmetic and copies ran while one was open for 0% -> 0% of each run, Pallas kernels for 23% -> 22%
where the time goes in v4:
time: 65.3 us; the launch traced here: 65 us
  waiting for transfers between devices  23.8 us (36%)
  Pallas kernels  20.2 us (31%)
  starting transfers between devices  19.1 us (29%)
  other arithmetic  0.96 us (1%)
  between operations  0.82 us (1%)
    ppermute x3, waiting for transfers between devices, local(): everyone.append(lax.ppermute(held, 'ep', far_by(bit)))  20.1 us
    ppermute x4, starting transfers between devices, local(): arrived.append(lax.ppermute(rows, ('ep', 'core'), pairs))  9.51 us
    pallas_call x1, Pallas kernels, local_recurrence(): pl.pallas_call(functools.partial(gates_kernel, first, count, len(weights)...  8.53 us
    pallas_call x1, Pallas kernels, add_carries(): pl.pallas_call(carry_kernel, grid=(channels // LANES,), in_specs=[pl.Bloc...  5.8 us
    all_to_all x1, starting transfers between devices, local(): lax.all_to_all(keep.reshape(experts * planes, capacity, model), ('ep', 'p...  4.84 us
    ppermute x3, starting transfers between devices, local(): everyone.append(lax.ppermute(held, 'ep', far_by(bit)))  4.49 us
    pallas_call x1, Pallas kernels, expert(): pl.pallas_call(functools.partial(expert_kernel, groups, cores), in_specs=...  3.5 us
    ppermute x1, waiting for transfers between devices, local(): other = lax.ppermute(arrived, 'core', swap)  1.9 us
  transfers between devices with their start and end apart: 10, of which 5 were waited for; matrix products, arithmetic and copies ran while one was open for 0% of the time, Pallas kernels for 22%

profile of v4, /device:TPU:0, one launch (start us, length us, event | category | flops | bytes accessed | tf_op | source)
XLA Modules:
  0.0 65.0 jit_solution(14321288225442205718)
XLA Ops:
  0.6 1.5 %prepare.1 = (bf16[2,16,64]{2,1,0:T(8,128)(2,1)S(1)}, bf16[32,2048]{1,0:T(8,128)(2,1)S(1)}, bf16[32,2048]{1,0:T(8,128)(2,1)S(1)}, bf16[32,2048]{1,0:T(8,128)(2,1)S(1)}, bf16[32,2048]{1,0:T(8,128)(2,1)S(1)}) custom-call(bf16[64,2048]{1,0:T(8,128)(2,1)} %in_ref.1, f32[1,2048]{1,0:T(1,128)} %bitcast.14, s32[2,64]{1,0:T(2,128)} %bitcast.15, f32[2,64]{1,0:T(2,128)} %bitcast.16), custom_call_target="tpu_custom_call" | custom-call | tf_op jit(solution)/shard_map/prepare/pallas_call | solution.py:481
  2.2 3.0 %collective-permute-start = (bf16[32,2048]{1,0:T(8,128)(2,1)S(1)}, bf16[32,2048]{1,0:T(8,128)(2,1)S(1)}, u32[]{:S(2)}, u32[]{:S(2)}) collective-permute-start(bf16[32,2048]{1,0:T(8,128)(2,1)S(1)} %get-tuple-element.26), channel_id=1, source_target_pairs={{0,4},{1,21},{4,0},{5,17},{8,12},{9,29},{12,8},{13,25},{16,20},{17... | collective-permute-start | bytes 393224 | tf_op jit(solution)/shard_map/ppermute | solution.py:602
  5.2 1.6 %collective-permute-start.1 = (bf16[32,2048]{1,0:T(8,128)(2,1)S(1)}, bf16[32,2048]{1,0:T(8,128)(2,1)S(1)}, u32[]{:S(2)}, u32[]{:S(2)}) collective-permute-start(bf16[32,2048]{1,0:T(8,128)(2,1)S(1)} %get-tuple-element.27), channel_id=1, source_target_pairs={{0,8},{1,25},{4,12},{5,29},{8,0},{9,17},{12,4},{13,21},{16,24},{17... | collective-permute-start | bytes 393224 | tf_op jit(solution)/shard_map/ppermute | solution.py:602
  6.8 0.0 collective-permute-start.2
  6.8 4.9 %collective-permute-start.3 = (bf16[32,2048]{1,0:T(8,128)(2,1)S(1)}, bf16[32,2048]{1,0:T(8,128)(2,1)S(1)}, u32[]{:S(2)}, u32[]{:S(2)}) collective-permute-start(bf16[32,2048]{1,0:T(8,128)(2,1)S(1)} %get-tuple-element.29), channel_id=1, source_target_pairs={{0,16},{1,1},{4,20},{5,5},{8,24},{9,9},{12,28},{13,13},{16,0},{17,... | collective-permute-start | bytes 393224 | tf_op jit(solution)/shard_map/ppermute | solution.py:602
  11.7 8.5 %recurrence.1 = (bf16[1024,512]{1,0:T(8,128)(2,1)S(1)}, bf16[1024,512]{1,0:T(8,128)(2,1)S(1)}, bf16[1024,512]{1,0:T(8,128)(2,1)S(1)}, f32[4,8,512]{2,1,0:T(8,128...) custom-call(bf16[1024,512]{1,0:T(8,128)(2,1)} %refs_0_.1, ...), custom_call_target="tpu_custom_call" | custom-call | tf_op jit(solution)/shard_map/recurrence/pallas_call | solution.py:223
  20.2 0.0 copy-start
  20.2 0.0 copy-start.1
  20.2 0.0 copy-start.2
  20.2 0.0 collective-permute-done
  20.3 0.0 collective-permute-done.1
  20.3 0.0 collective-permute-done.2
  20.3 0.0 collective-permute-done.3
  20.4 0.1 collective-permute-start.7
  20.4 1.9 %collective-permute-done.7.other_ref = bf16[128,2048]{1,0:T(8,128)(2,1)S(1)} collective-permute-done((bf16[128,2048]{1,0:T(8,128)(2,1)S(1)}, bf16[128,2048]{1,0:T(8,128)(2,1)S(1)}, u32[]{:S(2)}, u32[]{:S(2)}) %collective-permute-start.7) | collective-permute-done | bytes 524320 | tf_op jit(solution)/shard_map/ppermute | solution.py:617
  22.3 3.5 %experts.1 = (bf16[128,2048]{1,0:T(8,128)(2,1)S(1)}, bf16[128,2048]{1,0:T(8,128)(2,1)S(1)}) custom-call(bf16[128,2048]{1,0:T(8,128)(2,1)S(1)} %constant_dynamic-update-slice_fusion.own_ref, bf16[128,2048]{1,0:T(8,128)(2,1)S(1)} %collective-permute-done.7.other_ref, bf16[2048,1024]{1,0:T(8,128)(2,1)S(1)} %get-tuple-element.36.gate_ref, ...), custom_call_target="tpu_custom_call" | custom-call | tf_op jit(solution)/shard_map/experts/pallas_call | solution.py:529
  25.8 0.0 copy-done
  25.9 0.0 copy-done.1
  25.9 0.0 copy-done.2
  25.9 0.2 collective-permute-start.8
  26.1 1.8 %collective-permute-done.8 = bf16[128,2048]{1,0:T(8,128)(2,1)S(1)} collective-permute-done((bf16[128,2048]{1,0:T(8,128)(2,1)S(1)}, bf16[128,2048]{1,0:T(8,128)(2,1)S(1)}, u32[]{:S(2)}, u32[]{:S(2)}) %collective-permute-start.8) | collective-permute-done | bytes 524320 | tf_op jit(solution)/shard_map/ppermute | solution.py:625
  27.9 0.9 %fusion = bf16[16,8,2048]{2,1,0:T(8,128)(2,1)} fusion(bf16[128,2048]{1,0:T(8,128)(2,1)S(1)} %collective-permute-done.8, bf16[128,2048]{1,0:T(8,128)(2,1)S(1)} %get-tuple-element.39), kind=kLoop, calls=%fused_computation.1 | loop fusion | flops 1048576 | bytes 1572864 | tf_op jit(solution)/shard_map/reshape | solution.py:628
  28.8 4.8 %all-to-all-start = ((bf16[16,8,2048]{2,1,0:T(8,128)(2,1)}), bf16[16,8,2048]{2,1,0:T(8,128)(2,1)S(1)}, u32[]{:S(2)}, u32[]{:S(2)}) async-start(bf16[16,8,2048]{2,1,0:T(8,128)(2,1)} %fusion), calls=%async_computation | async-start | bytes 1048576 | tf_op jit(solution)/shard_map/all_to_all | solution.py:627
  33.6 2.9 %collective-permute-start.4 = (f32[1,3,4,512]{3,2,1,0:T(4,128)S(1)}, f32[1,3,4,512]{3,2,1,0:T(4,128)S(1)}, u32[]{:S(2)}, u32[]{:S(2)}) collective-permute-start(f32[1,3,4,512]{3,2,1,0:T(4,128)S(1)} %bitcast.9), channel_id=1, source_target_pairs={{0,16},{4,20},{8,24},{12,28},{16,0},{20,4},{24,8},{28,12},{1,17},{... | collective-permute-start | bytes 73736 | tf_op jit(solution)/shard_map/ppermute | solution.py:622
  36.5 12.8 %collective-permute-done.4.refs_1_ = f32[1,3,4,512]{3,2,1,0:T(4,128)S(1)} collective-permute-done((f32[1,3,4,512]{3,2,1,0:T(4,128)S(1)}, f32[1,3,4,512]{3,2,1,0:T(4,128)S(1)}, u32[]{:S(2)}, u32[]{:S(2)}) %collective-permute-start.4) | collective-permute-done | bytes 24608 | tf_op jit(solution)/shard_map/ppermute | solution.py:622
  49.4 0.1 collective-permute-start.5
  49.5 4.1 %collective-permute-done.5.refs_2_ = f32[2,3,4,512]{3,2,1,0:T(4,128)S(1)} collective-permute-done((f32[2,3,4,512]{3,2,1,0:T(4,128)S(1)}, f32[2,3,4,512]{3,2,1,0:T(4,128)S(1)}, u32[]{:S(2)}, u32[]{:S(2)}) %collective-permute-start.5) | collective-permute-done | bytes 49184 | tf_op jit(solution)/shard_map/ppermute | solution.py:622
  53.6 1.5 %collective-permute-start.6 = (f32[4,3,4,512]{3,2,1,0:T(4,128)S(1)}, f32[4,3,4,512]{3,2,1,0:T(4,128)S(1)}, u32[]{:S(2)}, u32[]{:S(2)}) collective-permute-start(f32[4,3,4,512]{3,2,1,0:T(4,128)S(1)} %pad_maximum_fusion), channel_id=1, source_target_pairs={{0,4},{4,0},{8,12},{12,8},{16,20},{20,16},{24,28},{28,24},{1,5},{5... | collective-permute-start | bytes 294920 | tf_op jit(solution)/shard_map/ppermute | solution.py:622
  55.1 3.2 %collective-permute-done.6.refs_3_ = f32[4,3,4,512]{3,2,1,0:T(4,128)S(1)} collective-permute-done((f32[4,3,4,512]{3,2,1,0:T(4,128)S(1)}, f32[4,3,4,512]{3,2,1,0:T(4,128)S(1)}, u32[]{:S(2)}, u32[]{:S(2)}) %collective-permute-start.6) | collective-permute-done | bytes 98336 | tf_op jit(solution)/shard_map/ppermute | solution.py:622
  58.3 5.8 %carries.1 = bf16[1024,512]{1,0:T(8,128)(2,1)} custom-call(bf16[1024,512]{1,0:T(8,128)(2,1)} %gate_ref.1, bf16[1024,512]{1,0:T(8,128)(2,1)} %copy-done, bf16[1024,512]{1,0:T(8,128)(2,1)} %copy-done.1, bf16[1024,512]{1,0:T(8,128)(2,1)} %copy-done.2, f32[4,8,512]{2,1,0:T(8,128)S(1)} %copy-done.4, f32[4,512]{1,0:T(4,128)} %taps_ref.1, ...), custom_call_target="tpu_custom_call" | custom-call | tf_op jit(solution)/shard_map/carries/pallas_call | solution.py:398
  64.1 0.0 all-to-all-done
  64.1 0.9 %combine.1 = bf16[16,2048]{1,0:T(8,128)(2,1)} custom-call(bf16[8,2,8,2048]{3,2,1,0:T(8,128)(2,1)S(1)} %bitcast.8, bf16[2,16,64]{2,1,0:T(8,128)(2,1)S(1)} %get-tuple-element.41.share_ref), custom_call_target="tpu_custom_call" | custom-call | tf_op jit(solution)/shard_map/combine/pallas_call | solution.py:553
  (10 shorter events, 0.1 us)
Async XLA Ops:
  2.2 18.1 %collective-permute-start = (bf16[32,2048]{1,0:T(8,128)(2,1)S(1)}, bf16[32,2048]{1,0:T(8,128)(2,1)S(1)}, u32[]{:S(2)}, u32[]{:S(2)}) collective-permute-start(bf16[32,2048]{1,0:T(8,128)(2,1)S(1)} %get-tuple-element.26), channel_id=1, source_target_pairs={{0,4},{1,21},{4,0},{5,17},{8,12},{9,29},{12,8},{13,25},{16,20},{17... | collective-permute-start | bytes 393224 | tf_op jit(solution)/shard_map/ppermute | solution.py:602
  5.2 15.1 %collective-permute-start.1 = (bf16[32,2048]{1,0:T(8,128)(2,1)S(1)}, bf16[32,2048]{1,0:T(8,128)(2,1)S(1)}, u32[]{:S(2)}, u32[]{:S(2)}) collective-permute-start(bf16[32,2048]{1,0:T(8,128)(2,1)S(1)} %get-tuple-element.27), channel_id=1, source_target_pairs={{0,8},{1,25},{4,12},{5,29},{8,0},{9,17},{12,4},{13,21},{16,24},{17... | collective-permute-start | bytes 393224 | tf_op jit(solution)/shard_map/ppermute | solution.py:602
  6.8 13.5 %collective-permute-start.2 = (bf16[32,2048]{1,0:T(8,128)(2,1)S(1)}, bf16[32,2048]{1,0:T(8,128)(2,1)S(1)}, u32[]{:S(2)}, u32[]{:S(2)}) collective-permute-start(bf16[32,2048]{1,0:T(8,128)(2,1)S(1)} %get-tuple-element.28), channel_id=1, source_target_pairs={{0,12},{1,29},{4,8},{5,25},{8,4},{9,21},{12,0},{13,17},{16,28},{17... | collective-permute-start | bytes 393224 | tf_op jit(solution)/shard_map/ppermute | solution.py:602
  6.8 13.5 %collective-permute-start.3 = (bf16[32,2048]{1,0:T(8,128)(2,1)S(1)}, bf16[32,2048]{1,0:T(8,128)(2,1)S(1)}, u32[]{:S(2)}, u32[]{:S(2)}) collective-permute-start(bf16[32,2048]{1,0:T(8,128)(2,1)S(1)} %get-tuple-element.29), channel_id=1, source_target_pairs={{0,16},{1,1},{4,20},{5,5},{8,24},{9,9},{12,28},{13,13},{16,0},{17,... | collective-permute-start | bytes 393224 | tf_op jit(solution)/shard_map/ppermute | solution.py:602
  20.2 5.6 %copy-start = (bf16[1024,512]{1,0:T(8,128)(2,1)}, bf16[1024,512]{1,0:T(8,128)(2,1)S(1)}, u32[]{:S(2)}) copy-start(bf16[1024,512]{1,0:T(8,128)(2,1)S(1)} %get-tuple-element.22.local_ref) | copy-start | bytes 3145732
  20.2 5.6 %copy-start.1 = (bf16[1024,512]{1,0:T(8,128)(2,1)}, bf16[1024,512]{1,0:T(8,128)(2,1)S(1)}, u32[]{:S(2)}) copy-start(bf16[1024,512]{1,0:T(8,128)(2,1)S(1)} %get-tuple-element.23.forward_ref) | copy-start | bytes 3145732
  20.2 5.6 %copy-start.2 = (bf16[1024,512]{1,0:T(8,128)(2,1)}, bf16[1024,512]{1,0:T(8,128)(2,1)S(1)}, u32[]{:S(2)}) copy-start(bf16[1024,512]{1,0:T(8,128)(2,1)S(1)} %get-tuple-element.24.backward_ref) | copy-start | bytes 3145732
  20.4 2.0 %collective-permute-start.7 = (bf16[128,2048]{1,0:T(8,128)(2,1)S(1)}, bf16[128,2048]{1,0:T(8,128)(2,1)S(1)}, u32[]{:S(2)}, u32[]{:S(2)}) collective-permute-start(bf16[128,2048]{1,0:T(8,128)(2,1)S(1)} %constant_dynamic-update-slice_fusion.own_ref), channel_id=1, source_target_pairs={{0,1},{1,0},{2,3},{3,2},{4,5},{5,4},{6,7},{7,6},{8,9},{9,8},{10,11... | collective-permute-start | bytes 1572872 | tf_op jit(solution)/shard_map/ppermute | solution.py:617
  22.3 11.3 %copy-start.3 = (f32[3,4,512]{2,1,0:T(4,128)S(1)}, f32[3,4,512]{2,1,0:T(4,128)}, u32[]{:S(2)}) copy-start(f32[3,4,512]{2,1,0:T(4,128)} %get-tuple-element.31) | copy-start | bytes 73732
  22.3 35.9 %copy-start.4 = (f32[4,8,512]{2,1,0:T(8,128)S(1)}, f32[4,8,512]{2,1,0:T(8,128)}, u32[]{:S(2)}) copy-start(f32[4,8,512]{2,1,0:T(8,128)} %get-tuple-element.25.chunk_ref) | copy-start | bytes 196612
  25.9 2.0 %collective-permute-start.8 = (bf16[128,2048]{1,0:T(8,128)(2,1)S(1)}, bf16[128,2048]{1,0:T(8,128)(2,1)S(1)}, u32[]{:S(2)}, u32[]{:S(2)}) collective-permute-start(bf16[128,2048]{1,0:T(8,128)(2,1)S(1)} %get-tuple-element.40), channel_id=1, source_target_pairs={{0,1},{1,0},{2,3},{3,2},{4,5},{5,4},{6,7},{7,6},{8,9},{9,8},{10,11... | collective-permute-start | bytes 1572872 | tf_op jit(solution)/shard_map/ppermute | solution.py:625
  28.8 35.3 %all-to-all-start = ((bf16[16,8,2048]{2,1,0:T(8,128)(2,1)}), bf16[16,8,2048]{2,1,0:T(8,128)(2,1)S(1)}, u32[]{:S(2)}, u32[]{:S(2)}) async-start(bf16[16,8,2048]{2,1,0:T(8,128)(2,1)} %fusion), calls=%async_computation | async-start | bytes 1048576 | tf_op jit(solution)/shard_map/all_to_all | solution.py:627
  33.6 15.7 %collective-permute-start.4 = (f32[1,3,4,512]{3,2,1,0:T(4,128)S(1)}, f32[1,3,4,512]{3,2,1,0:T(4,128)S(1)}, u32[]{:S(2)}, u32[]{:S(2)}) collective-permute-start(f32[1,3,4,512]{3,2,1,0:T(4,128)S(1)} %bitcast.9), channel_id=1, source_target_pairs={{0,16},{4,20},{8,24},{12,28},{16,0},{20,4},{24,8},{28,12},{1,17},{... | collective-permute-start | bytes 73736 | tf_op jit(solution)/shard_map/ppermute | solution.py:622
  49.4 4.2 %collective-permute-start.5 = (f32[2,3,4,512]{3,2,1,0:T(4,128)S(1)}, f32[2,3,4,512]{3,2,1,0:T(4,128)S(1)}, u32[]{:S(2)}, u32[]{:S(2)}) collective-permute-start(f32[2,3,4,512]{3,2,1,0:T(4,128)S(1)} %pad_maximum_fusion.1), channel_id=1, source_target_pairs={{0,8},{4,12},{8,0},{12,4},{16,24},{20,28},{24,16},{28,20},{1,9},{5... | collective-permute-start | bytes 147464 | tf_op jit(solution)/shard_map/ppermute | solution.py:622
  53.6 4.7 %collective-permute-start.6 = (f32[4,3,4,512]{3,2,1,0:T(4,128)S(1)}, f32[4,3,4,512]{3,2,1,0:T(4,128)S(1)}, u32[]{:S(2)}, u32[]{:S(2)}) collective-permute-start(f32[4,3,4,512]{3,2,1,0:T(4,128)S(1)} %pad_maximum_fusion), channel_id=1, source_target_pairs={{0,4},{4,0},{8,12},{12,8},{16,20},{20,16},{24,28},{28,24},{1,5},{5... | collective-permute-start | bytes 294920 | tf_op jit(solution)/shard_map/ppermute | solution.py:622
